TPU v7x, 512 devices: a whole 4x8x8 slice. The times are simulated.
512 devices in a mesh: sp: 256 (over z, y, x), tp: 2 (over core).
Axes of the slice: x: 4, y: 8, z: 8, core: 2. Of those that a mesh axis runs over, the one named last changes fastest.
Arguments:
- features: bfloat16 [65536, 1024], P('sp', 'tp'), may hold values from -6 to 6
- lambda_real: float32 [64, 64], P('tp'), may hold values from -4 to 0, as said below
- lambda_imag: float32 [64, 64], P('tp'), may hold values from 0.5 to 201.06177
- log_step: float32 [64], P('tp'), may hold values from -5 to -2
- input_real: float32 [64, 64, 16], P('tp'), may hold values from -0.5 to 0.5
- input_imag: float32 [64, 64, 16], P('tp'), may hold values from -0.5 to 0.5
- real_output: float32 [64, 16, 64], P('tp'), may hold values from -0.75 to 0.75
- imaginary_output: float32 [64, 16, 64], P('tp'), may hold values from -0.75 to 0.75
- skip_gain: float32 [1024], P('tp'), may hold values from -4 to 4
- value_weight: bfloat16 [1024, 2048], P('tp'), may hold values from -0.1875 to 0.1875
- gate_weight: bfloat16 [1024, 2048], P('tp'), may hold values from -0.1875 to 0.1875
- value_bias: float32 [2048], replicated, may hold values from -3 to 3
- gate_bias: float32 [2048], replicated, may hold values from -3 to 3
Outputs:
- mixed_output: bfloat16 [65536, 2048], P(('sp', 'tp'))
Inputs may be any that keep to these rules, and one draw needn't show every extreme that they name: `lambda_real`: negative.
All inputs are finite; a program needn't handle non-finite values.
Results may differ from a plain program's by a relative error of at most 0.03.
Values may be sent and summed in bfloat16 or wider, within the bound.
A program may use at most 128 MiB of HBM per device.

v0:
```python
import functools

import jax
import jax.numpy as jnp
from jax import lax
from jax.experimental import pallas as pl
from jax.experimental.pallas import tpu as pltpu
from jax.sharding import PartitionSpec as P

MESH = pl.DeviceIdType.MESH
F32 = jnp.float32
BF16 = jnp.bfloat16


def iota(shape, dim):
    return lax.broadcasted_iota(jnp.int32, shape, dim)


def cmul(ar, ai, br, bi):
    return ar * br - ai * bi, ar * bi + ai * br


def nt_dot(left, right):
    return lax.dot_general(left, right, (((1,), (1,)), ((), ())), preferred_element_type=F32)


def kernel(nsp, ntp, dims, *refs):
    rows, groups, state, size, width = dims
    (x_h, lr_h, li_h, ls_h, br_h, bi_h, cr_h, ci_h, sk_h, vw_h, gw_h, vb_h, gb_h, out_ref,
     x_v, lr_v, li_v, ls_v, br_v, bi_v, cr_v, ci_v, sk_v, vw_v, gw_v, vb_v, gb_v,
     xp_v, zr_v, zi_v, zcat_v, wcat_v, crm_v, cim_v, resp_v, act_v,
     hx_v, fin_v, a_all_v, msg_v, recv_v, h_v, part_v, inbox_v,
     in_sem, send_sem, recv_sem, psend_sem, precv_sem) = refs
    me = lax.axis_index("sp")
    core = lax.axis_index("tp")
    gpb = 128 // size
    lanes = gpb * state
    blocks = groups // gpb
    chunks = 16
    length = rows // chunks
    own_rows = rows // ntp

    hbm = (ls_h, lr_h, li_h, x_h, br_h, bi_h, cr_h, ci_h, sk_h, vb_h, gb_h, vw_h, gw_h)
    vmem = (ls_v, lr_v, li_v, x_v, br_v, bi_v, cr_v, ci_v, sk_v, vb_v, gb_v, vw_v, gw_v)
    copies = [pltpu.make_async_copy(s, d, in_sem.at[i]) for i, (s, d) in enumerate(zip(hbm, vmem))]
    for c in copies[:6]:
        c.start()

    barrier = pltpu.get_barrier_semaphore()
    for k in range(1, ntp):
        pl.semaphore_signal(barrier, inc=1, device_id=(me, lax.rem(core + k, ntp)), device_id_type=MESH)

    @pl.loop(1, nsp)
    def _(k):
        pl.semaphore_signal(barrier, inc=1, device_id=(lax.rem(me + k, nsp), core), device_id_type=MESH)

    for c in copies[:3]:
        c.wait()
    eye = iota((groups, groups), 0) == iota((groups, groups), 1)
    step = jnp.exp(jnp.sum(jnp.where(eye, ls_v[...], 0.0), axis=1, keepdims=True))
    lam_r, lam_i = lr_v[...], li_v[...]
    mag = jnp.exp(lam_r * step)
    phase = lam_i * step
    t_r, t_i = mag * jnp.cos(phase), mag * jnp.sin(phase)
    den = lam_r * lam_r + lam_i * lam_i
    n_r = t_r - 1.0
    f_r = (n_r * lam_r + t_i * lam_i) / den
    f_i = (t_i * lam_r - n_r * lam_i) / den

    per = 128 // state
    row8, lane8 = iota((gpb, 128), 0), iota((gpb, 128), 1)

    def flat(value, b):
        sub = value[b * gpb:(b + 1) * gpb]
        dup = jnp.concatenate([sub] * per, axis=1)
        return jnp.concatenate(
            [jnp.sum(jnp.where(row8 == per * j + lane8 // state, dup, 0.0), axis=0, keepdims=True)
             for j in range(gpb // per)], axis=1)

    r0, r1 = iota((rows, rows), 0), iota((rows, rows), 1)
    shuffle = jnp.where(r1 == (r0 % chunks) * length + r0 // chunks, 1.0, 0.0).astype(BF16)
    copies[3].wait()
    xp_v[...] = jnp.dot(shuffle, x_v[...], preferred_element_type=F32).astype(BF16)


    c_mask = iota((128, lanes), 0) // size == iota((128, lanes), 1) // state

    def diagonal(tall):
        return jnp.where(c_mask, jnp.concatenate([tall] * gpb, axis=1), 0.0)

    copies[4].wait()
    copies[5].wait()
    for c in copies[6:]:
        c.start()
    crow = iota((chunks, lanes), 0)

    def shift(value, s):
        return jnp.where(crow >= s, pltpu.roll(value, s, 0), 0.0)

    for b in range(blocks):
        xb = xp_v[:, b * 128:(b + 1) * 128]

        def inject(ref):
            mat = diagonal(ref[b * gpb:(b + 1) * gpb].reshape(128, state)).astype(BF16)
            return jnp.dot(xb, mat, preferred_element_type=F32)

        zr_v[b] = inject(br_v)
        zi_v[b] = inject(bi_v)
        a1r, a1i = flat(t_r, b), flat(t_i, b)
        ar, ai = jnp.broadcast_to(a1r, (chunks, lanes)), jnp.broadcast_to(a1i, (chunks, lanes))
        z_r = z_i = None
        for o in range(length):
            here = pl.ds(o * chunks, chunks)
            if o == 0:
                z_r, z_i = zr_v[b, here, :], zi_v[b, here, :]
            else:
                p_r, p_i = cmul(ar, ai, z_r, z_i)
                z_r, z_i = p_r + zr_v[b, here, :], p_i + zi_v[b, here, :]
                zr_v[b, here, :] = z_r
                zi_v[b, here, :] = z_i
        qr, qi = ar, ai
        s = 1
        while s < length:
            qr, qi = cmul(qr, qi, qr, qi)
            s *= 2
        pw_r, pw_i = jnp.ones_like(qr), jnp.zeros_like(qr)
        s = 1
        while s < chunks:
            m_r, m_i = cmul(qr, qi, shift(z_r, s), shift(z_i, s))
            z_r, z_i = z_r + m_r, z_i + m_i
            bit = (crow // s) % 2 == 1
            pw_r, pw_i = cmul(pw_r, pw_i, jnp.where(bit, qr, 1.0), jnp.where(bit, qi, 0.0))
            qr, qi = cmul(qr, qi, qr, qi)
            s *= 2
        hx_v[0, b], hx_v[1, b] = shift(z_r, 1), shift(z_i, 1)
        fin_v[b:b + 1] = z_r[chunks - 1:]
        fin_v[blocks + b:blocks + b + 1] = z_i[chunks - 1:]
        a_all_v[b:b + 1] = qr[:1]
        a_all_v[blocks + b:blocks + b + 1] = qi[:1]
        hx_v[2, b], hx_v[3, b] = pw_r, pw_i
    msg_v[...] = fin_v[...].astype(BF16)

    pl.semaphore_wait(barrier, nsp - 1 + ntp - 1)

    def outgoing(d):
        return pltpu.make_async_remote_copy(
            src_ref=msg_v, dst_ref=recv_v.at[me], send_sem=send_sem.at[d], recv_sem=recv_sem.at[me],
            device_id=(d, core), device_id_type=MESH)

    @pl.loop(me + 1, nsp)
    def _(d):
        outgoing(d).start()

    copies[6].wait()
    copies[7].wait()
    copies[8].wait()
    for b in range(blocks):
        a1r, a1i = flat(t_r, b), flat(t_i, b)
        ar, ai = jnp.broadcast_to(a1r, (chunks, lanes)), jnp.broadcast_to(a1i, (chunks, lanes))
        w_r, w_i = hx_v[0, b], hx_v[1, b]
        p_r, p_i = hx_v[2, b], hx_v[3, b]
        for o in range(length):
            here = pl.ds(o * chunks, chunks)
            w_r, w_i = cmul(ar, ai, w_r, w_i)
            p_r, p_i = cmul(ar, ai, p_r, p_i)
            zcat_v[here, :lanes] = (zr_v[b, here, :] + w_r).astype(BF16)
            zcat_v[here, lanes:] = (zi_v[b, here, :] + w_i).astype(BF16)
            wcat_v[b, here, :lanes] = p_r.astype(BF16)
            wcat_v[b, here, lanes:] = p_i.astype(BF16)
        gains_r, gains_i = [], []
        for g in range(b * gpb, (b + 1) * gpb):
            g_r, g_i = cmul(cr_v[g], ci_v[g], f_r[g:g + 1], f_i[g:g + 1])
            gains_r.append(g_r)
            gains_i.append(g_i)

        m_r = diagonal(jnp.concatenate(gains_r, axis=0))
        m_i = diagonal(jnp.concatenate(gains_i, axis=0))
        crm_v[b], cim_v[b] = m_r, m_i
        mats = jnp.concatenate([m_r.astype(BF16), (-m_i).astype(BF16)], axis=1)
        col = pl.ds(b * 128, 128)
        resp_v[:, col] = nt_dot(zcat_v[...], mats) + sk_v[:, col] * xp_v[:, col].astype(F32)

    A_r, A_i = a_all_v[:blocks], a_all_v[blocks:]
    zero = jnp.zeros((blocks, lanes), F32)

    def gather(k, carry):
        h_r, h_i, p_r, p_i = carry
        d = me - 1 - k
        pltpu.make_async_remote_copy(
            src_ref=msg_v, dst_ref=recv_v.at[d], send_sem=send_sem.at[d], recv_sem=recv_sem.at[d],
            device_id=(d, core), device_id_type=MESH).wait_recv()
        got = recv_v[d].astype(F32)
        m_r, m_i = cmul(p_r, p_i, got[:blocks], got[blocks:])
        return (h_r + m_r, h_i + m_i) + cmul(p_r, p_i, A_r, A_i)

    h_r, h_i, _, _ = lax.fori_loop(0, me, gather, (zero, zero, zero + 1.0, zero))
    h_v[:blocks] = h_r
    h_v[blocks:] = h_i

    for b in range(blocks):
        k_r, k_i = cmul(crm_v[b], cim_v[b], h_v[b:b + 1], h_v[blocks + b:blocks + b + 1])
        mats = jnp.concatenate([k_r.astype(BF16), (-k_i).astype(BF16)], axis=1)
        col = pl.ds(b * 128, 128)
        total = resp_v[:, col] + nt_dot(wcat_v[b], mats)
        act_v[:, col] = jax.nn.gelu(total).astype(BF16)

    back = jnp.where(r1 == (r0 % length) * chunks + r0 // length, 1.0, 0.0).astype(BF16)
    act = jnp.dot(back, act_v[...], preferred_element_type=F32).astype(BF16)

    for c in copies[9:]:
        c.wait()
    piece = inbox_v.shape[-1]
    pieces = width // piece

    def exchange(j, k):
        to = lax.rem(core + k, ntp)
        return pltpu.make_async_remote_copy(
            src_ref=part_v.at[j, to], dst_ref=inbox_v.at[j, k - 1],
            send_sem=psend_sem.at[j, k - 1], recv_sem=precv_sem.at[j, k - 1],
            device_id=(me, to), device_id_type=MESH)

    for j in range(pieces):
        col = pl.ds(j * piece, piece)
        for which, weight in enumerate((vw_v, gw_v)):
            part = jnp.dot(act, weight[:, col], preferred_element_type=F32).astype(BF16)
            for i in range(ntp):
                part_v[j, i, which] = part[i * own_rows:(i + 1) * own_rows]
        for k in range(1, ntp):
            exchange(j, k).start()
    for j in range(pieces):
        col = pl.ds(j * piece, piece)
        for k in range(1, ntp):
            exchange(j, k).wait_recv()
        sums = []
        for which, bias in enumerate((vb_v, gb_v)):
            total = part_v[j, core, which].astype(F32)
            for k in range(1, ntp):
                total = total + inbox_v[j, k - 1, which].astype(F32)
            sums.append(total + bias[:, col])
        out_ref[:, col] = (sums[0] * jax.nn.sigmoid(sums[1])).astype(BF16)
    for j in range(pieces):
        for k in range(1, ntp):
            exchange(j, k).wait_send()

    @pl.loop(me + 1, nsp)
    def _(d):
        outgoing(d).wait_send()


def local(nsp, ntp, features, lambda_real, lambda_imag, log_step, input_real, input_imag, real_output,
          imaginary_output, skip_gain, value_weight, gate_weight, value_bias, gate_bias):
    rows, channels = features.shape
    groups, state = lambda_real.shape
    size = input_real.shape[2]
    input_real, input_imag = jnp.swapaxes(input_real, 1, 2), jnp.swapaxes(input_imag, 1, 2)
    width = value_weight.shape[1]
    gpb = 128 // size
    lanes, blocks, chunks = gpb * state, groups // gpb, 16
    piece = min(512, width)
    args = (features, lambda_real, lambda_imag, log_step[None], input_real, input_imag, real_output,
            imaginary_output, skip_gain[None], value_weight, gate_weight, value_bias[None], gate_bias[None])
    scratch = [pltpu.VMEM(a.shape, a.dtype) for a in args]
    scratch += [
        pltpu.VMEM((rows, channels), BF16),
        pltpu.VMEM((blocks, rows, lanes), F32),
        pltpu.VMEM((blocks, rows, lanes), F32),
        pltpu.VMEM((rows, 2 * lanes), BF16),
        pltpu.VMEM((blocks, rows, 2 * lanes), BF16),
        pltpu.VMEM((blocks, 128, lanes), F32),
        pltpu.VMEM((blocks, 128, lanes), F32),
        pltpu.VMEM((rows, channels), F32),
        pltpu.VMEM((rows, channels), BF16),
        pltpu.VMEM((4, blocks, chunks, lanes), F32),
        pltpu.VMEM((2 * blocks, lanes), F32),
        pltpu.VMEM((2 * blocks, lanes), F32),
        pltpu.VMEM((2 * blocks, lanes), BF16),
        pltpu.VMEM((nsp, 2 * blocks, lanes), BF16),
        pltpu.VMEM((2 * blocks, lanes), F32),
        pltpu.VMEM((width // piece, ntp, 2, rows // ntp, piece), BF16),
        pltpu.VMEM((width // piece, ntp - 1, 2, rows // ntp, piece), BF16),
        pltpu.SemaphoreType.DMA((len(args),)),
        pltpu.SemaphoreType.DMA((nsp,)),
        pltpu.SemaphoreType.DMA((nsp,)),
        pltpu.SemaphoreType.DMA((width // piece, ntp - 1)),
        pltpu.SemaphoreType.DMA((width // piece, ntp - 1)),
    ]
    return pl.pallas_call(
        functools.partial(kernel, nsp, ntp, (rows, groups, state, size, width)),
        out_shape=pltpu.VMEM((rows // ntp, width), BF16),
        in_specs=[pl.BlockSpec(memory_space=pl.ANY)] * len(args),
        out_specs=pl.BlockSpec(memory_space=pltpu.VMEM),
        scratch_shapes=scratch,
        compiler_params=pltpu.CompilerParams(
            collective_id=0, has_side_effects=True, vmem_limit_bytes=60 * 1024 * 1024),
        name="mixer",
    )(*args)


def solution(mesh):
    in_specs = (
        P("sp", "tp"),
        P("tp", None),
        P("tp", None),
        P("tp"),
        P("tp", None, None),
        P("tp", None, None),
        P("tp", None, None),
        P("tp", None, None),
        P("tp"),
        P("tp", None),
        P("tp", None),
        P(),
        P(),
    )
    out_specs = P(("sp", "tp"), None)
    body = functools.partial(local, mesh.shape["sp"], mesh.shape["tp"])
    return jax.shard_map(body, mesh=mesh, in_specs=in_specs, out_specs=out_specs, check_vma=False)
```

profile of v0, /device:TPU:505, one launch (start us, length us, event | category | flops | bytes accessed | tf_op | source)
XLA Modules:
  0.0 90.8 jit_solution(16245158226455047731)
XLA Ops:
  0.0 90.0 %mixer.1 = bf16[128,2048]{1,0:T(8,128)(2,1)S(1)} custom-call(bf16[256,512]{1,0:T(8,128)(2,1)} %refs_0_.1, f32[32,64]{1,0:T(8,128)} %refs_1_.1, f32[32,64]{1,0:T(8,128)} %refs_2_.1, f32[1,32]{1,0:T(1,128)} %bitcast.11, f32[32,16,64]{2,1,0:T(8,128)} %bitcast.6, f32[32,16,64]{2,1,0:T(8,128)} %bitcast.7, f32[32,16,64]{2,1,0:T(8,128)} %refs_6_.1, ...), custom_call_target="tpu_custom_call" | custom-call | tf_op jit(solution)/shard_map/mixer/pallas_call | solution.py:287
  90.0 0.8 copy.15
where the time goes:
time: 90.9 us; the launch traced here: 90.8 us
  Pallas kernels  90 us (99%)
    pallas_call x1, Pallas kernels, local(): pl.pallas_call(functools.partial(kernel, nsp, ntp, (rows, groups, state,...  90 us

commit v1 on v0

--- a/solution.py
+++ b/solution.py
@@ -24,21 +24,31 @@
     return lax.dot_general(left, right, (((1,), (1,)), ((), ())), preferred_element_type=F32)
 
 
-def kernel(nsp, ntp, dims, *refs):
+def split_ring(nsp):
+    nx = min(8, nsp)
+    ny = min(8, nsp // nx)
+    return nsp // (nx * ny), ny, nx
+
+
+def kernel(ring, ntp, dims, *refs):
+    nz, ny, nx = ring
     rows, groups, state, size, width = dims
     (x_h, lr_h, li_h, ls_h, br_h, bi_h, cr_h, ci_h, sk_h, vw_h, gw_h, vb_h, gb_h, out_ref,
      x_v, lr_v, li_v, ls_v, br_v, bi_v, cr_v, ci_v, sk_v, vw_v, gw_v, vb_v, gb_v,
      xp_v, zr_v, zi_v, zcat_v, wcat_v, crm_v, cim_v, resp_v, act_v,
-     hx_v, fin_v, a_all_v, msg_v, recv_v, h_v, part_v, inbox_v,
-     in_sem, send_sem, recv_sem, psend_sem, precv_sem) = refs
+     hx_v, fin_v, a_all_v, tab_x, tab_y, msg_v, recv_x, recv_y, recv_z, h_v, part_v, inbox_v,
+     in_sem, send_x, got_x, send_y, got_y, send_z, got_z, psend_sem, precv_sem) = refs
     me = lax.axis_index("sp")
     core = lax.axis_index("tp")
+    x, y, z = lax.rem(me, nx), lax.rem(me // nx, ny), me // (nx * ny)
     gpb = 128 // size
     lanes = gpb * state
     blocks = groups // gpb
     chunks = 16
     length = rows // chunks
     own_rows = rows // ntp
+    tall, wide = fin_v.shape[0] // 2, fin_v.shape[1]
+    fold = lanes // wide
 
     hbm = (ls_h, lr_h, li_h, x_h, br_h, bi_h, cr_h, ci_h, sk_h, vb_h, gb_h, vw_h, gw_h)
     vmem = (ls_v, lr_v, li_v, x_v, br_v, bi_v, cr_v, ci_v, sk_v, vb_v, gb_v, vw_v, gw_v)
@@ -50,9 +60,14 @@
     for k in range(1, ntp):
         pl.semaphore_signal(barrier, inc=1, device_id=(me, lax.rem(core + k, ntp)), device_id_type=MESH)
 
-    @pl.loop(1, nsp)
-    def _(k):
-        pl.semaphore_signal(barrier, inc=1, device_id=(lax.rem(me + k, nsp), core), device_id_type=MESH)
+    def peer(at, count, stride, k):
+        other = lax.rem(at + k, count)
+        return other, (me + (other - at) * stride, core)
+
+    lines = ((x, nx, 1), (y, ny, nx), (z, nz, nx * ny))
+    for line in lines:
+        for k in range(1, line[1]):
+            pl.semaphore_signal(barrier, inc=1, device_id=peer(*line, k)[1], device_id_type=MESH)
 
     for c in copies[:3]:
         c.wait()
@@ -133,28 +148,70 @@
             qr, qi = cmul(qr, qi, qr, qi)
             s *= 2
         hx_v[0, b], hx_v[1, b] = shift(z_r, 1), shift(z_i, 1)
-        fin_v[b:b + 1] = z_r[chunks - 1:]
-        fin_v[blocks + b:blocks + b + 1] = z_i[chunks - 1:]
-        a_all_v[b:b + 1] = qr[:1]
-        a_all_v[blocks + b:blocks + b + 1] = qi[:1]
+        for ref, val_r, val_i in ((fin_v, z_r[chunks - 1:], z_i[chunks - 1:]), (a_all_v, qr[:1], qi[:1])):
+            for u in range(fold):
+                at, cols = b * fold + u, slice(u * wide, (u + 1) * wide)
+                ref[at:at + 1] = val_r[:, cols]
+                ref[tall + at:tall + at + 1] = val_i[:, cols]
         hx_v[2, b], hx_v[3, b] = pw_r, pw_i
-    msg_v[...] = fin_v[...].astype(BF16)
-
-    pl.semaphore_wait(barrier, nsp - 1 + ntp - 1)
-
-    def outgoing(d):
+    msg_v[0] = fin_v[...].astype(BF16)
+
+    pl.semaphore_wait(barrier, nx - 1 + ny - 1 + nz - 1 + ntp - 1)
+
+    def outgoing(stage, k):
+        at = lines[stage][0]
+        other, device = peer(*lines[stage], k)
         return pltpu.make_async_remote_copy(
-            src_ref=msg_v, dst_ref=recv_v.at[me], send_sem=send_sem.at[d], recv_sem=recv_sem.at[me],
-            device_id=(d, core), device_id_type=MESH)
-
-    @pl.loop(me + 1, nsp)
-    def _(d):
-        outgoing(d).start()
+            src_ref=msg_v.at[stage], dst_ref=(recv_x, recv_y, recv_z)[stage].at[at],
+            send_sem=(send_x, send_y, send_z)[stage].at[other], recv_sem=(got_x, got_y, got_z)[stage].at[at],
+            device_id=device, device_id_type=MESH)
+
+    def incoming(stage, k):
+        other, device = peer(*lines[stage], k)
+        recv = (recv_x, recv_y, recv_z)[stage].at[other]
+        pltpu.make_async_remote_copy(
+            src_ref=msg_v.at[stage], dst_ref=recv,
+            send_sem=(send_x, send_y, send_z)[stage].at[other], recv_sem=(got_x, got_y, got_z)[stage].at[other],
+            device_id=device, device_id_type=MESH).wait_recv()
+        got = recv[...].astype(F32)
+        return other, got[:tall], got[tall:]
+
+    def near_first(count):
+        return sorted(range(1, count), key=lambda k: min(k, count - k))
+
+    for k in reversed(near_first(nx)):
+        outgoing(0, k).start()
+
+    def powers(tab, count, a_r, a_i):
+        p_r, p_i = jnp.ones((tall, wide), F32), jnp.zeros((tall, wide), F32)
+        for i in range(count):
+            tab[i] = jnp.zeros((2 * tall, wide), F32)
+            tab[count + i, :tall], tab[count + i, tall:] = p_r, p_i
+            p_r, p_i = cmul(p_r, p_i, a_r, a_i)
+        return p_r, p_i
+
+    ax_r, ax_i = powers(tab_x, nx, a_all_v[:tall], a_all_v[tall:])
+    ay_r, ay_i = powers(tab_y, ny, ax_r, ax_i)
+
+    def weight(tab, at, v_r, v_i):
+        return cmul(tab[at, :tall], tab[at, tall:], v_r, v_i)
+
+    def collect(stage, tab, own_r, own_i):
+        at, count, _ = lines[stage]
+        t_r, t_i = weight(tab, count + count - 1 - at, own_r, own_i)
+        p_r = p_i = jnp.zeros((tall, wide), F32)
+        for k in near_first(count):
+            other, v_r, v_i = incoming(stage, k)
+            m_r, m_i = weight(tab, count + count - 1 - other, v_r, v_i)
+            t_r, t_i = t_r + m_r, t_i + m_i
+            m_r, m_i = weight(tab, count + at - 1 - other, v_r, v_i)
+            p_r, p_i = p_r + m_r, p_i + m_i
+        return t_r, t_i, p_r, p_i
 
     copies[6].wait()
     copies[7].wait()
     copies[8].wait()
-    for b in range(blocks):
+    def respond(b):
         a1r, a1i = flat(t_r, b), flat(t_i, b)
         ar, ai = jnp.broadcast_to(a1r, (chunks, lanes)), jnp.broadcast_to(a1i, (chunks, lanes))
         w_r, w_i = hx_v[0, b], hx_v[1, b]
@@ -180,25 +237,41 @@
         col = pl.ds(b * 128, 128)
         resp_v[:, col] = nt_dot(zcat_v[...], mats) + sk_v[:, col] * xp_v[:, col].astype(F32)
 
-    A_r, A_i = a_all_v[:blocks], a_all_v[blocks:]
-    zero = jnp.zeros((blocks, lanes), F32)
+    half = blocks // 2
+    for b in range(half):
+        respond(b)
+    row_r, row_i, hx_r, hx_i = collect(0, tab_x, fin_v[:tall], fin_v[tall:])
+    msg_v[1, :tall], msg_v[1, tall:] = row_r.astype(BF16), row_i.astype(BF16)
+    for k in reversed(near_first(ny)):
+        outgoing(1, k).start()
+    for b in range(half, blocks):
+        respond(b)
+    plane_r, plane_i, hy_r, hy_i = collect(1, tab_y, row_r, row_i)
+    msg_v[2, :tall], msg_v[2, tall:] = plane_r.astype(BF16), plane_i.astype(BF16)
+
+    @pl.loop(z + 1, nz)
+    def _(d):
+        outgoing(2, d - z).start()
+
+    m_r, m_i = weight(tab_x, nx + x, hy_r, hy_i)
+    h_r, h_i = hx_r + m_r, hx_i + m_i
+    s_r, s_i = weight(tab_x, nx + x, tab_y[ny + y, :tall], tab_y[ny + y, tall:])
 
     def gather(k, carry):
         h_r, h_i, p_r, p_i = carry
-        d = me - 1 - k
-        pltpu.make_async_remote_copy(
-            src_ref=msg_v, dst_ref=recv_v.at[d], send_sem=send_sem.at[d], recv_sem=recv_sem.at[d],
-            device_id=(d, core), device_id_type=MESH).wait_recv()
-        got = recv_v[d].astype(F32)
-        m_r, m_i = cmul(p_r, p_i, got[:blocks], got[blocks:])
-        return (h_r + m_r, h_i + m_i) + cmul(p_r, p_i, A_r, A_i)
-
-    h_r, h_i, _, _ = lax.fori_loop(0, me, gather, (zero, zero, zero + 1.0, zero))
-    h_v[:blocks] = h_r
-    h_v[blocks:] = h_i
+        _, v_r, v_i = incoming(2, nz - 1 - k)
+        m_r, m_i = cmul(p_r, p_i, v_r, v_i)
+        return (h_r + m_r, h_i + m_i) + cmul(p_r, p_i, ay_r, ay_i)
+
+    h_r, h_i, _, _ = lax.fori_loop(0, z, gather, (h_r, h_i, s_r, s_i))
+    h_v[:tall] = h_r
+    h_v[tall:] = h_i
+
+    def flat_h(at, b):
+        return jnp.concatenate([h_v[at + b * fold + u:at + b * fold + u + 1] for u in range(fold)], axis=1)
 
     for b in range(blocks):
-        k_r, k_i = cmul(crm_v[b], cim_v[b], h_v[b:b + 1], h_v[blocks + b:blocks + b + 1])
+        k_r, k_i = cmul(crm_v[b], cim_v[b], flat_h(0, b), flat_h(tall, b))
         mats = jnp.concatenate([k_r.astype(BF16), (-k_i).astype(BF16)], axis=1)
         col = pl.ds(b * 128, 128)
         total = resp_v[:, col] + nt_dot(wcat_v[b], mats)
@@ -242,9 +315,13 @@
         for k in range(1, ntp):
             exchange(j, k).wait_send()
 
-    @pl.loop(me + 1, nsp)
+    for stage in range(2):
+        for k in range(1, lines[stage][1]):
+            outgoing(stage, k).wait_send()
+
+    @pl.loop(z + 1, nz)
     def _(d):
-        outgoing(d).wait_send()
+        outgoing(2, d - z).wait_send()
 
 
 def local(nsp, ntp, features, lambda_real, lambda_imag, log_step, input_real, input_imag, real_output,
@@ -257,6 +334,8 @@
     gpb = 128 // size
     lanes, blocks, chunks = gpb * state, groups // gpb, 16
     piece = min(512, width)
+    ring = nz, ny, nx = split_ring(nsp)
+    held = (16, 2 * blocks * lanes // 16)
     args = (features, lambda_real, lambda_imag, log_step[None], input_real, input_imag, real_output,
             imaginary_output, skip_gain[None], value_weight, gate_weight, value_bias[None], gate_bias[None])
     scratch = [pltpu.VMEM(a.shape, a.dtype) for a in args]
@@ -271,21 +350,29 @@
         pltpu.VMEM((rows, channels), F32),
         pltpu.VMEM((rows, channels), BF16),
         pltpu.VMEM((4, blocks, chunks, lanes), F32),
-        pltpu.VMEM((2 * blocks, lanes), F32),
-        pltpu.VMEM((2 * blocks, lanes), F32),
-        pltpu.VMEM((2 * blocks, lanes), BF16),
-        pltpu.VMEM((nsp, 2 * blocks, lanes), BF16),
-        pltpu.VMEM((2 * blocks, lanes), F32),
+        pltpu.VMEM(held, F32),
+        pltpu.VMEM(held, F32),
+        pltpu.VMEM((2 * nx,) + held, F32),
+        pltpu.VMEM((2 * ny,) + held, F32),
+        pltpu.VMEM((3,) + held, BF16),
+        pltpu.VMEM((nx,) + held, BF16),
+        pltpu.VMEM((ny,) + held, BF16),
+        pltpu.VMEM((nz,) + held, BF16),
+        pltpu.VMEM(held, F32),
         pltpu.VMEM((width // piece, ntp, 2, rows // ntp, piece), BF16),
         pltpu.VMEM((width // piece, ntp - 1, 2, rows // ntp, piece), BF16),
         pltpu.SemaphoreType.DMA((len(args),)),
-        pltpu.SemaphoreType.DMA((nsp,)),
-        pltpu.SemaphoreType.DMA((nsp,)),
+        pltpu.SemaphoreType.DMA((nx,)),
+        pltpu.SemaphoreType.DMA((nx,)),
+        pltpu.SemaphoreType.DMA((ny,)),
+        pltpu.SemaphoreType.DMA((ny,)),
+        pltpu.SemaphoreType.DMA((nz,)),
+        pltpu.SemaphoreType.DMA((nz,)),
         pltpu.SemaphoreType.DMA((width // piece, ntp - 1)),
         pltpu.SemaphoreType.DMA((width // piece, ntp - 1)),
     ]
     return pl.pallas_call(
-        functools.partial(kernel, nsp, ntp, (rows, groups, state, size, width)),
+        functools.partial(kernel, ring, ntp, (rows, groups, state, size, width)),
         out_shape=pltpu.VMEM((rows // ntp, width), BF16),
         in_specs=[pl.BlockSpec(memory_space=pl.ANY)] * len(args),
         out_specs=pl.BlockSpec(memory_space=pltpu.VMEM),

time: 90.9 us -> 30.6 us (0.34)
  the two profiles are of different devices: /device:TPU:505 before, /device:TPU:1 now
where the time goes in v1:
time: 30.6 us; the launch traced here: 30.5 us
  Pallas kernels  29.7 us (97%)
  local copies, waits for them, and re-layouts  0.8 us (3%)
    pallas_call x1, Pallas kernels, local(): pl.pallas_call(functools.partial(kernel, ring, ntp, (rows, groups, state,...  29.7 us
    unnamed x1, local copies, waits for them, and re-layouts  0.8 us

profile of v1, /device:TPU:1, one launch (start us, length us, event | category | flops | bytes accessed | tf_op | source)
XLA Modules:
  0.0 30.5 jit_solution(1929896221261721838)
XLA Ops:
  0.0 29.7 %mixer.1 = bf16[128,2048]{1,0:T(8,128)(2,1)S(1)} custom-call(bf16[256,512]{1,0:T(8,128)(2,1)} %refs_0_.1, f32[32,64]{1,0:T(8,128)} %refs_1_.1, f32[32,64]{1,0:T(8,128)} %refs_2_.1, f32[1,32]{1,0:T(1,128)} %bitcast.11, f32[32,16,64]{2,1,0:T(8,128)} %bitcast.6, f32[32,16,64]{2,1,0:T(8,128)} %bitcast.7, f32[32,16,64]{2,1,0:T(8,128)} %refs_6_.1, ...), custom_call_target="tpu_custom_call" | custom-call | tf_op jit(solution)/shard_map/mixer/pallas_call | solution.py:374
  29.7 0.8 %copy.15 = bf16[128,2048]{1,0:T(8,128)(2,1)} copy(bf16[128,2048]{1,0:T(8,128)(2,1)S(1)} %mixer.1) | data formatting | bytes 1048576

commit v2 on v1

--- a/solution.py
+++ b/solution.py
@@ -25,7 +25,7 @@
 
 
 def split_ring(nsp):
-    nx = min(8, nsp)
+    nx = min(4, nsp)
     ny = min(8, nsp // nx)
     return nsp // (nx * ny), ny, nx
 
@@ -37,7 +37,7 @@
      x_v, lr_v, li_v, ls_v, br_v, bi_v, cr_v, ci_v, sk_v, vw_v, gw_v, vb_v, gb_v,
      xp_v, zr_v, zi_v, zcat_v, wcat_v, crm_v, cim_v, resp_v, act_v,
      hx_v, fin_v, a_all_v, tab_x, tab_y, msg_v, recv_x, recv_y, recv_z, h_v, part_v, inbox_v,
-     in_sem, send_x, got_x, send_y, got_y, send_z, got_z, psend_sem, precv_sem) = refs
+     in_sem, send_x, got_x, send_y, got_y, send_z, got_z, ready, psend_sem, precv_sem) = refs
     me = lax.axis_index("sp")
     core = lax.axis_index("tp")
     x, y, z = lax.rem(me, nx), lax.rem(me // nx, ny), me // (nx * ny)
@@ -65,9 +65,13 @@
         return other, (me + (other - at) * stride, core)
 
     lines = ((x, nx, 1), (y, ny, nx), (z, nz, nx * ny))
-    for line in lines:
+    for line in lines[:2]:
         for k in range(1, line[1]):
             pl.semaphore_signal(barrier, inc=1, device_id=peer(*line, k)[1], device_id_type=MESH)
+
+    @pl.loop(z + 1, nz)
+    def _(d):
+        pl.semaphore_signal(barrier, inc=1, device_id=peer(*lines[2], d - z)[1], device_id_type=MESH)
 
     for c in copies[:3]:
         c.wait()
@@ -156,7 +160,11 @@
         hx_v[2, b], hx_v[3, b] = pw_r, pw_i
     msg_v[0] = fin_v[...].astype(BF16)
 
-    pl.semaphore_wait(barrier, nx - 1 + ny - 1 + nz - 1 + ntp - 1)
+    pl.semaphore_wait(barrier, nx - 1 + ny - 1 + ntp - 1 + z)
+
+    @pl.loop(0, z)
+    def _(d):
+        pl.semaphore_signal(ready.at[z], inc=1, device_id=peer(*lines[2], d - z + nz)[1], device_id_type=MESH)
 
     def outgoing(stage, k):
         at = lines[stage][0]
@@ -251,6 +259,7 @@
 
     @pl.loop(z + 1, nz)
     def _(d):
+        pl.semaphore_wait(ready.at[d], 1)
         outgoing(2, d - z).start()
 
     m_r, m_i = weight(tab_x, nx + x, hy_r, hy_i)
@@ -368,6 +377,7 @@
         pltpu.SemaphoreType.DMA((ny,)),
         pltpu.SemaphoreType.DMA((nz,)),
         pltpu.SemaphoreType.DMA((nz,)),
+        pltpu.SemaphoreType.REGULAR((nz,)),
         pltpu.SemaphoreType.DMA((width // piece, ntp - 1)),
         pltpu.SemaphoreType.DMA((width // piece, ntp - 1)),
     ]

time: 30.6 us -> 24.2 us (0.79)
  the two profiles are of different devices: /device:TPU:1 before, /device:TPU:449 now
where the time goes in v2:
time: 24.2 us; the launch traced here: 24.1 us
  Pallas kernels  23.3 us (96%)
  local copies, waits for them, and re-layouts  0.8 us (3%)
    pallas_call x1, Pallas kernels, local(): pl.pallas_call(functools.partial(kernel, ring, ntp, (rows, groups, state,...  23.3 us
    unnamed x1, local copies, waits for them, and re-layouts  0.8 us

profile of v2, /device:TPU:449, one launch (start us, length us, event | category | flops | bytes accessed | tf_op | source)
XLA Modules:
  0.0 24.1 jit_solution(16005231968494194928)
XLA Ops:
  0.0 23.3 %mixer.1 = bf16[128,2048]{1,0:T(8,128)(2,1)S(1)} custom-call(bf16[256,512]{1,0:T(8,128)(2,1)} %refs_0_.1, f32[32,64]{1,0:T(8,128)} %refs_1_.1, f32[32,64]{1,0:T(8,128)} %refs_2_.1, f32[1,32]{1,0:T(1,128)} %bitcast.11, f32[32,16,64]{2,1,0:T(8,128)} %bitcast.6, f32[32,16,64]{2,1,0:T(8,128)} %bitcast.7, f32[32,16,64]{2,1,0:T(8,128)} %refs_6_.1, ...), custom_call_target="tpu_custom_call" | custom-call | tf_op jit(solution)/shard_map/mixer/pallas_call | solution.py:384
  23.3 0.8 %copy.15 = bf16[128,2048]{1,0:T(8,128)(2,1)} copy(bf16[128,2048]{1,0:T(8,128)(2,1)S(1)} %mixer.1) | data formatting | bytes 1048576

commit v3 on v2

v3 whole, which is shorter than its diff:
```python
import functools

import jax
import jax.numpy as jnp
from jax import lax
from jax.experimental import pallas as pl
from jax.experimental.pallas import tpu as pltpu
from jax.sharding import PartitionSpec as P

MESH = pl.DeviceIdType.MESH
F32 = jnp.float32
BF16 = jnp.bfloat16


def iota(shape, dim):
    return lax.broadcasted_iota(jnp.int32, shape, dim)


def cmul(ar, ai, br, bi):
    return ar * br - ai * bi, ar * bi + ai * br


def nt_dot(left, right):
    return lax.dot_general(left, right, (((1,), (1,)), ((), ())), preferred_element_type=F32)


def split_ring(nsp):
    nx = min(4, nsp)
    ny = min(8, nsp // nx)
    return nsp // (nx * ny), ny, nx


def near_first(count):
    return sorted(range(1, count), key=lambda k: min(k, count - k))


def kernel(ring, ntp, dims, *refs):
    nz, ny, nx = ring
    rows, groups, state, size, width = dims
    (x_h, lr_h, li_h, ls_h, br_h, bi_h, cr_h, ci_h, sk_h, vw_h, gw_h, vb_h, gb_h, out_ref,
     x_v, lr_v, li_v, ls_v, br_v, bi_v, cr_v, ci_v, sk_v, vb_v, gb_v, w_v,
     xp_v, bmat_v, mats_v, zr_v, zi_v, zcat_v, wcat_v, gain_v, resp_v, corr_v, act_v, part_v,
     par_v, fin_v, tab_x, tab_y, msg_v, recv_x, recv_y, recv_z, h_v,
     in_sem, w_sem, send_x, got_x, send_y, got_y, send_z, got_z, ready, w_send, w_got, a_send, a_got) = refs
    me = lax.axis_index("sp")
    core = lax.axis_index("tp")
    other_core = 1 - core
    x, y, z = lax.rem(me, nx), lax.rem(me // nx, ny), me // (nx * ny)
    gpb = 128 // size
    lanes = gpb * state
    blocks = groups // gpb
    chunks = 16
    length = rows // chunks
    half = rows // ntp
    tall, wide = fin_v.shape[0] // 2, fin_v.shape[1]
    fold = lanes // wide
    per = 128 // state

    hbm = (x_h, ls_h, lr_h, li_h, br_h, bi_h, cr_h, ci_h, sk_h, vb_h, gb_h)
    vmem = (x_v, ls_v, lr_v, li_v, br_v, bi_v, cr_v, ci_v, sk_v, vb_v, gb_v)
    copies = [pltpu.make_async_copy(s, d, in_sem.at[i]) for i, (s, d) in enumerate(zip(hbm, vmem))]
    for c in copies:
        c.start()
    weights = (vw_h, gw_h)
    own_w = [pltpu.make_async_copy(s, w_v.at[i, core], w_sem.at[i]) for i, s in enumerate(weights)]
    peer_w = [pltpu.make_async_remote_copy(
        src_ref=s, dst_ref=w_v.at[i, core], send_sem=w_send.at[i], recv_sem=w_got.at[i],
        device_id=(me, other_core), device_id_type=MESH) for i, s in enumerate(weights)]
    got_w = [pltpu.make_async_remote_copy(
        src_ref=s, dst_ref=w_v.at[i, other_core], send_sem=w_send.at[i], recv_sem=w_got.at[i],
        device_id=(me, other_core), device_id_type=MESH) for i, s in enumerate(weights)]

    barrier = pltpu.get_barrier_semaphore()
    pl.semaphore_signal(barrier, inc=1, device_id=(me, other_core), device_id_type=MESH)

    def peer(at, count, stride, k):
        other = lax.rem(at + k, count)
        return other, (me + (other - at) * stride, core)

    lines = ((x, nx, 1), (y, ny, nx), (z, nz, nx * ny))
    for line in lines[:2]:
        for k in range(1, line[1]):
            pl.semaphore_signal(barrier, inc=1, device_id=peer(*line, k)[1], device_id_type=MESH)

    @pl.loop(z + 1, nz)
    def _(d):
        pl.semaphore_signal(barrier, inc=1, device_id=peer(*lines[2], d - z)[1], device_id_type=MESH)

    bmat_v[...] = jnp.zeros_like(bmat_v)
    pair_mask = [iota((size, 128), 1) // state == i for i in range(per)]

    def spread(value, g):
        return jnp.where(pair_mask[g % per], jnp.concatenate([value] * per, axis=1), 0.0)

    for c in copies[1:4]:
        c.wait()
    eye = iota((groups, groups), 0) == iota((groups, groups), 1)
    step = jnp.exp(jnp.sum(jnp.where(eye, ls_v[...], 0.0), axis=1, keepdims=True))
    lam_r, lam_i = lr_v[...], li_v[...]
    mag = jnp.exp(lam_r * step)
    phase = lam_i * step
    t_r, t_i = mag * jnp.cos(phase), mag * jnp.sin(phase)
    den = lam_r * lam_r + lam_i * lam_i
    n_r = t_r - 1.0
    f_r = (n_r * lam_r + t_i * lam_i) / den
    f_i = (t_i * lam_r - n_r * lam_i) / den

    row8, lane8 = iota((gpb, 128), 0), iota((gpb, 128), 1)

    def hold(at, value):
        for b in range(blocks):
            dup = jnp.concatenate([value[b * gpb:(b + 1) * gpb]] * per, axis=1)
            for j in range(gpb // per):
                tile = jnp.sum(jnp.where(row8 == per * j + lane8 // state, dup, 0.0), axis=0, keepdims=True)
                flat = j * 128
                r, c = b * fold + flat // wide, flat % wide
                par_v[at, r:r + 1, c:c + 128] = tile

    hold(0, t_r)
    hold(1, t_i)
    hold(2, f_r)
    hold(3, f_i)

    def pair(k):
        return par_v[2 * k], par_v[2 * k + 1]

    q_r, q_i = pair(0)
    squares = rows.bit_length() - 1
    for k in range(squares):
        q_r, q_i = cmul(q_r, q_i, q_r, q_i)
        par_v[4 + 2 * k] = q_r
        par_v[5 + 2 * k] = q_i

    def row(k, b):
        return [jnp.concatenate([par_v[2 * k + i, b * fold + u:b * fold + u + 1] for u in range(fold)], axis=1)
                for i in range(2)]

    def power(exponent, b):
        return row(0 if exponent == 1 else exponent.bit_length(), b)

    row_b = iota((8, lanes), 0)

    def eight(b, flip):
        count = 7 - row_b if flip else row_b
        v_r, v_i = jnp.ones((8, lanes), F32), jnp.zeros((8, lanes), F32)
        for k in range(3):
            bit = (count // (1 << k)) % 2 == 1
            s_r, s_i = power(1 << k, b)
            v_r, v_i = cmul(v_r, v_i, jnp.where(bit, s_r, 1.0), jnp.where(bit, s_i, 0.0))
        return v_r, v_i

    copies[4].wait()
    copies[5].wait()
    for g in range(groups):
        b, l = g // gpb, g % gpb
        at, cols = slice(l * size, (l + 1) * size), l // per * 128
        bmat_v[b, at, cols:cols + 128] = spread(br_v[g], g).astype(BF16)
        bmat_v[b, at, lanes + cols:lanes + cols + 128] = spread(bi_v[g], g).astype(BF16)
    copies[0].wait()

    def inject(source, b):
        out = jnp.dot(source[:, b * 128:(b + 1) * 128], bmat_v[b], preferred_element_type=F32)
        zr_v[b] = out[:, :lanes]
        zi_v[b] = out[:, lanes:]

    for b in range(blocks):
        inject(x_v, b)
    for b in range(blocks):
        e_r, e_i = power(8, b)
        ends = []
        steps = rows // 16
        for h in range(2):
            z_r, z_i = zr_v[b, h * half:h * half + 8, :], zi_v[b, h * half:h * half + 8, :]
            for k in range(1, steps):
                here = pl.ds(h * half + 8 * k, 8)
                p_r, p_i = cmul(e_r, e_i, z_r, z_i)
                z_r, z_i = p_r + zr_v[b, here, :], p_i + zi_v[b, here, :]
            ends.append((z_r, z_i))
        p_r, p_i = cmul(*power(rows // 2, b), *ends[0])
        v_r, v_i = cmul(*eight(b, True), p_r + ends[1][0], p_i + ends[1][1])
        v_r, v_i = jnp.sum(v_r, axis=0, keepdims=True), jnp.sum(v_i, axis=0, keepdims=True)
        for u in range(fold):
            at, cols = b * fold + u, slice(u * wide, (u + 1) * wide)
            fin_v[at:at + 1] = v_r[:, cols]
            fin_v[tall + at:tall + at + 1] = v_i[:, cols]
    msg_v[0] = fin_v[...].astype(BF16)

    pl.semaphore_wait(barrier, nx - 1 + ny - 1 + ntp - 1 + z)

    def outgoing(stage, k):
        at = lines[stage][0]
        other, device = peer(*lines[stage], k)
        return pltpu.make_async_remote_copy(
            src_ref=msg_v.at[stage], dst_ref=(recv_x, recv_y, recv_z)[stage].at[at],
            send_sem=(send_x, send_y, send_z)[stage].at[other], recv_sem=(got_x, got_y, got_z)[stage].at[at],
            device_id=device, device_id_type=MESH)

    def incoming(stage, k):
        other, device = peer(*lines[stage], k)
        recv = (recv_x, recv_y, recv_z)[stage].at[other]
        pltpu.make_async_remote_copy(
            src_ref=msg_v.at[stage], dst_ref=recv,
            send_sem=(send_x, send_y, send_z)[stage].at[other], recv_sem=(got_x, got_y, got_z)[stage].at[other],
            device_id=device, device_id_type=MESH).wait_recv()
        got = recv[...].astype(F32)
        return other, got[:tall], got[tall:]

    for k in reversed(near_first(nx)):
        outgoing(0, k).start()

    @pl.loop(0, z)
    def _(d):
        pl.semaphore_signal(ready.at[z], inc=1, device_id=peer(*lines[2], d - z + nz)[1], device_id_type=MESH)

    for c in own_w + peer_w:
        c.start()

    def powers(tab, count, a_r, a_i):
        p_r, p_i = jnp.ones((tall, wide), F32), jnp.zeros((tall, wide), F32)
        for i in range(count):
            tab[i] = jnp.zeros((2 * tall, wide), F32)
            tab[count + i, :tall], tab[count + i, tall:] = p_r, p_i
            p_r, p_i = cmul(p_r, p_i, a_r, a_i)
        return p_r, p_i

    ax_r, ax_i = powers(tab_x, nx, q_r, q_i)
    ay_r, ay_i = powers(tab_y, ny, ax_r, ax_i)

    def weight(tab, at, v_r, v_i):
        return cmul(tab[at, :tall], tab[at, tall:], v_r, v_i)

    def collect(stage, tab, own_r, own_i):
        at, count, _ = lines[stage]
        t_r, t_i = weight(tab, count + count - 1 - at, own_r, own_i)
        p_r = p_i = jnp.zeros((tall, wide), F32)
        for k in near_first(count):
            other, v_r, v_i = incoming(stage, k)
            m_r, m_i = weight(tab, count + count - 1 - other, v_r, v_i)
            t_r, t_i = t_r + m_r, t_i + m_i
            m_r, m_i = weight(tab, count + at - 1 - other, v_r, v_i)
            p_r, p_i = p_r + m_r, p_i + m_i
        return t_r, t_i, p_r, p_i

    mats_v[...] = jnp.zeros_like(mats_v)
    r0, r1 = iota((rows, rows), 0), iota((rows, rows), 1)
    shuffle = jnp.where(r1 == (r0 % chunks) * length + r0 // chunks, 1.0, 0.0).astype(BF16)
    back = jnp.where(r1 == (r0 % length) * chunks + r0 // length, 1.0, 0.0).astype(BF16)
    xp_v[...] = jnp.dot(shuffle, x_v[...], preferred_element_type=F32).astype(BF16)
    crow = iota((chunks, lanes), 0)

    def shift(value, s):
        return jnp.where(crow >= s, pltpu.roll(value, s, 0), 0.0)

    copies[6].wait()
    copies[7].wait()
    copies[8].wait()

    def place(b, slot, l, v_r, v_i):
        at, cols = slot * 128 + l * size, l // per * 128
        mats_v[b, at:at + size, cols:cols + 128] = v_r.astype(BF16)
        mats_v[b, at:at + size, lanes + cols:lanes + cols + 128] = (-v_i).astype(BF16)

    def respond(b):
        inject(xp_v, b)
        a_r, a_i = power(1, b)
        z_r, z_i = zr_v[b, :chunks, :], zi_v[b, :chunks, :]
        for o in range(1, length):
            here = pl.ds(o * chunks, chunks)
            p_r, p_i = cmul(a_r, a_i, z_r, z_i)
            z_r, z_i = p_r + zr_v[b, here, :], p_i + zi_v[b, here, :]
            zr_v[b, here, :] = z_r
            zi_v[b, here, :] = z_i
        s = 1
        while s < chunks:
            m_r, m_i = cmul(*power(length * s, b), shift(z_r, s), shift(z_i, s))
            z_r, z_i = z_r + m_r, z_i + m_i
            s *= 2
        w_r, w_i = shift(z_r, 1), shift(z_i, 1)
        for o in range(length):
            here = pl.ds(o * chunks, chunks)
            w_r, w_i = cmul(a_r, a_i, w_r, w_i)
            zcat_v[b, here, :lanes] = (zr_v[b, here, :] + w_r).astype(BF16)
            zcat_v[b, here, lanes:] = (zi_v[b, here, :] + w_i).astype(BF16)
        e_r, e_i = power(8, b)
        v_r, v_i = cmul(a_r, a_i, *eight(b, False))
        for o in range(half // 16):
            n_r, n_i = cmul(e_r, e_i, v_r, v_i)
            here = pl.ds(o * 16, 16)
            wcat_v[b, here, :lanes] = jnp.concatenate([v_r, n_r], axis=0).astype(BF16)
            wcat_v[b, here, lanes:] = jnp.concatenate([v_i, n_i], axis=0).astype(BF16)
            v_r, v_i = cmul(e_r, e_i, n_r, n_i)
        g_r, g_i = row(1, b)
        for l in range(gpb):
            g, cols = b * gpb + l, slice(l // per * 128, l // per * 128 + 128)
            c_r, c_i = cmul(spread(cr_v[g], g), spread(ci_v[g], g), g_r[:, cols], g_i[:, cols])
            gain_v[0, g], gain_v[1, g] = c_r, c_i
            place(b, 0, l, c_r, c_i)
        col = pl.ds(b * 128, 128)
        out = nt_dot(zcat_v[b], mats_v[b, :128])
        high = out.astype(BF16)
        low = (out - high.astype(F32)).astype(BF16)
        turned = jnp.dot(back, jnp.concatenate([high, low], axis=1), preferred_element_type=F32)
        resp_v[:, col] = turned[:, :128] + turned[:, 128:] + sk_v[:, col] * x_v[:, col].astype(F32)

    for b in range(blocks // 2):
        respond(b)
    row_r, row_i, hx_r, hx_i = collect(0, tab_x, fin_v[:tall], fin_v[tall:])
    msg_v[1, :tall], msg_v[1, tall:] = row_r.astype(BF16), row_i.astype(BF16)
    for k in reversed(near_first(ny)):
        outgoing(1, k).start()
    for b in range(blocks // 2, blocks):
        respond(b)
    plane_r, plane_i, hy_r, hy_i = collect(1, tab_y, row_r, row_i)
    msg_v[2, :tall], msg_v[2, tall:] = plane_r.astype(BF16), plane_i.astype(BF16)

    @pl.loop(z + 1, nz)
    def _(d):
        pl.semaphore_wait(ready.at[d], 1)
        outgoing(2, d - z).start()

    m_r, m_i = weight(tab_x, nx + x, hy_r, hy_i)
    h_r, h_i = hx_r + m_r, hx_i + m_i
    s_r, s_i = weight(tab_x, nx + x, tab_y[ny + y, :tall], tab_y[ny + y, tall:])

    def gather(k, carry):
        h_r, h_i, p_r, p_i = carry
        _, v_r, v_i = incoming(2, nz - 1 - k)
        m_r, m_i = cmul(p_r, p_i, v_r, v_i)
        return (h_r + m_r, h_i + m_i) + cmul(p_r, p_i, ay_r, ay_i)

    h_r, h_i, _, _ = lax.fori_loop(0, z, gather, (h_r, h_i, s_r, s_i))
    late_r, late_i = cmul(*pair(1 + (half.bit_length() - 1)), h_r, h_i)
    for slot, is_late in enumerate((core == 0, core == 1)):
        h_v[slot, :tall] = jnp.where(is_late, late_r, h_r)
        h_v[slot, tall:] = jnp.where(is_late, late_i, h_i)

    def start_of(who):
        return pl.multiple_of(who * half, half)

    for b in range(blocks):
        for slot in range(ntp):
            for l in range(gpb):
                g, flat = b * gpb + l, l // per * 128
                r, cols = b * fold + flat // wide, slice(flat % wide, flat % wide + 128)
                place(b, 1 + slot, l, *cmul(
                    gain_v[0, g], gain_v[1, g], h_v[slot, r:r + 1, cols], h_v[slot, tall + r:tall + r + 1, cols]))
        col = pl.ds(b * 128, 128)
        corr = nt_dot(wcat_v[b], mats_v[b, 128:])
        corr_v[:, col] = corr[:, 128:]
        act_v[0, :, col] = jax.nn.gelu(corr[:, :128] + resp_v[pl.ds(start_of(other_core), half), col]).astype(BF16)
    exchange = pltpu.make_async_remote_copy(
        src_ref=act_v.at[0], dst_ref=act_v.at[2], send_sem=a_send, recv_sem=a_got,
        device_id=(me, other_core), device_id_type=MESH)
    exchange.start()
    act_v[1] = jax.nn.gelu(corr_v[...] + resp_v[pl.ds(start_of(core), half), :]).astype(BF16)
    copies[9].wait()
    copies[10].wait()
    for c in own_w:
        c.wait()
    piece = min(512, width)
    cols_of = [pl.ds(j * piece, piece) for j in range(width // piece)]
    for col in cols_of:
        for i in range(2):
            part_v[i, :, col] = jnp.dot(act_v[1], w_v[i, core, :, col], preferred_element_type=F32)
    for c in got_w:
        c.wait_recv()
    exchange.wait_recv()
    for col in cols_of:
        sums = [part_v[i, :, col] + bias[:, col]
                + jnp.dot(act_v[2], w_v[i, other_core, :, col], preferred_element_type=F32)
                for i, bias in enumerate((vb_v, gb_v))]
        out_ref[:, col] = (sums[0] * jax.nn.sigmoid(sums[1])).astype(BF16)
    exchange.wait_send()
    for c in peer_w:
        c.wait_send()
    for stage in range(2):
        for k in range(1, lines[stage][1]):
            outgoing(stage, k).wait_send()

    @pl.loop(z + 1, nz)
    def _(d):
        outgoing(2, d - z).wait_send()


def local(nsp, ntp, features, lambda_real, lambda_imag, log_step, input_real, input_imag, real_output,
          imaginary_output, skip_gain, value_weight, gate_weight, value_bias, gate_bias):
    rows, channels = features.shape
    groups, state = lambda_real.shape
    size = input_real.shape[2]
    input_real, input_imag = jnp.swapaxes(input_real, 1, 2), jnp.swapaxes(input_imag, 1, 2)
    width = value_weight.shape[1]
    gpb = 128 // size
    lanes, blocks = gpb * state, groups // gpb
    ring = nz, ny, nx = split_ring(nsp)
    held = (16, 2 * blocks * lanes // 16)
    single = (8, held[1])
    half = rows // ntp
    args = (features, lambda_real, lambda_imag, log_step[None], input_real, input_imag, real_output,
            imaginary_output, skip_gain[None], value_weight, gate_weight, value_bias[None], gate_bias[None])
    scratch = [pltpu.VMEM(a.shape, a.dtype) for a in args[:9] + args[11:]]
    scratch += [
        pltpu.VMEM((2, ntp, channels, width), BF16),
        pltpu.VMEM((rows, channels), BF16),
        pltpu.VMEM((blocks, 128, 2 * lanes), BF16),
        pltpu.VMEM((blocks, 3 * 128, 2 * lanes), BF16),
        pltpu.VMEM((blocks, rows, lanes), F32),
        pltpu.VMEM((blocks, rows, lanes), F32),
        pltpu.VMEM((blocks, rows, 2 * lanes), BF16),
        pltpu.VMEM((blocks, half, 2 * lanes), BF16),
        pltpu.VMEM((2, groups, size, 128), F32),
        pltpu.VMEM((rows, channels), F32),
        pltpu.VMEM((half, channels), F32),
        pltpu.VMEM((3, half, channels), BF16),
        pltpu.VMEM((2, half, width), F32),
        pltpu.VMEM((4 + 2 * (rows.bit_length() - 1),) + single, F32),
        pltpu.VMEM(held, F32),
        pltpu.VMEM((2 * nx,) + held, F32),
        pltpu.VMEM((2 * ny,) + held, F32),
        pltpu.VMEM((3,) + held, BF16),
        pltpu.VMEM((nx,) + held, BF16),
        pltpu.VMEM((ny,) + held, BF16),
        pltpu.VMEM((nz,) + held, BF16),
        pltpu.VMEM((ntp,) + held, F32),
        pltpu.SemaphoreType.DMA((11,)),
        pltpu.SemaphoreType.DMA((2,)),
        pltpu.SemaphoreType.DMA((nx,)),
        pltpu.SemaphoreType.DMA((nx,)),
        pltpu.SemaphoreType.DMA((ny,)),
        pltpu.SemaphoreType.DMA((ny,)),
        pltpu.SemaphoreType.DMA((nz,)),
        pltpu.SemaphoreType.DMA((nz,)),
        pltpu.SemaphoreType.REGULAR((nz,)),
        pltpu.SemaphoreType.DMA((2,)),
        pltpu.SemaphoreType.DMA((2,)),
        pltpu.SemaphoreType.DMA,
        pltpu.SemaphoreType.DMA,
    ]
    return pl.pallas_call(
        functools.partial(kernel, ring, ntp, (rows, groups, state, size, width)),
        out_shape=pltpu.VMEM((rows // ntp, width), BF16),
        in_specs=[pl.BlockSpec(memory_space=pl.ANY)] * len(args),
        out_specs=pl.BlockSpec(memory_space=pltpu.VMEM),
        scratch_shapes=scratch,
        compiler_params=pltpu.CompilerParams(
            collective_id=0, has_side_effects=True, vmem_limit_bytes=60 * 1024 * 1024),
        name="mixer",
    )(*args)


def solution(mesh):
    in_specs = (
        P("sp", "tp"),
        P("tp", None),
        P("tp", None),
        P("tp"),
        P("tp", None, None),
        P("tp", None, None),
        P("tp", None, None),
        P("tp", None, None),
        P("tp"),
        P("tp", None),
        P("tp", None),
        P(),
        P(),
    )
    out_specs = P(("sp", "tp"), None)
    body = functools.partial(local, mesh.shape["sp"], mesh.shape["tp"])
    return jax.shard_map(body, mesh=mesh, in_specs=in_specs, out_specs=out_specs, check_vma=False)
```

time: 24.2 us -> 22.5 us (0.930)
  the two profiles are of different devices: /device:TPU:449 before, /device:TPU:1 now
where the time goes in v3:
time: 22.5 us; the launch traced here: 22.1 us
  Pallas kernels  21.3 us (95%)
  local copies, waits for them, and re-layouts  0.8 us (4%)
    pallas_call x1, Pallas kernels, local(): pl.pallas_call(functools.partial(kernel, ring, ntp, (rows, groups, state,...  21.3 us
    unnamed x1, local copies, waits for them, and re-layouts  0.8 us

profile of v3, /device:TPU:1, one launch (start us, length us, event | category | flops | bytes accessed | tf_op | source)
XLA Modules:
  0.0 22.1 jit_solution(8094867571182365928)
XLA Ops:
  0.0 21.3 %mixer.1 = bf16[128,2048]{1,0:T(8,128)(2,1)S(1)} custom-call(bf16[256,512]{1,0:T(8,128)(2,1)} %refs_0_.1, f32[32,64]{1,0:T(8,128)} %refs_1_.1, f32[32,64]{1,0:T(8,128)} %refs_2_.1, f32[1,32]{1,0:T(1,128)} %bitcast.11, f32[32,16,64]{2,1,0:T(8,128)} %bitcast.6, f32[32,16,64]{2,1,0:T(8,128)} %bitcast.7, f32[32,16,64]{2,1,0:T(8,128)} %refs_6_.1, ...), custom_call_target="tpu_custom_call" | custom-call | tf_op jit(solution)/shard_map/mixer/pallas_call | solution.py:438
  21.3 0.8 %copy.15 = bf16[128,2048]{1,0:T(8,128)(2,1)} copy(bf16[128,2048]{1,0:T(8,128)(2,1)S(1)} %mixer.1) | data formatting | bytes 1048576

commit v4 on v3

v4 whole, which is shorter than its diff:
```python
import functools

import jax
import jax.numpy as jnp
from jax import lax
from jax.experimental import pallas as pl
from jax.experimental.pallas import tpu as pltpu
from jax.sharding import PartitionSpec as P

MESH = pl.DeviceIdType.MESH
F32 = jnp.float32
BF16 = jnp.bfloat16


def iota(shape, dim):
    return lax.broadcasted_iota(jnp.int32, shape, dim)


def cmul(ar, ai, br, bi):
    return ar * br - ai * bi, ar * bi + ai * br


def nt_dot(left, right):
    return lax.dot_general(left, right, (((1,), (1,)), ((), ())), preferred_element_type=F32)


def split_ring(nsp):
    nx = min(4, nsp)
    ny = min(8, nsp // nx)
    return nsp // (nx * ny), ny, nx


def near_first(count):
    return sorted(range(1, count), key=lambda k: min(k, count - k))


def kernel(ring, ntp, dims, *refs):
    nz, ny, nx = ring
    rows, groups, state, size, width = dims
    (x_h, lr_h, li_h, ls_h, br_h, bi_h, cr_h, ci_h, sk_h, vw_h, gw_h, vb_h, gb_h, out_ref,
     x_v, lr_v, li_v, ls_v, br_v, bi_v, cr_v, ci_v, sk_v, vb_v, gb_v, w_v,
     xp_v, bmat_v, mats_v, keep_v, zr_v, zi_v, zcat_v, wcat_v, gain_v, resp_v, both_v, act_v,
     par_v, fin_v, tab_x, tab_y, sum_v, end_v, row_v, plane_v, recv_x, recv_y, recv_z, h_v, pass_v,
     in_sem, w_sem, send_x, got_x, send_y, got_y, send_z, got_z, ready, d_send, d_got) = refs
    me = lax.axis_index("sp")
    core = lax.axis_index("tp")
    other_core = 1 - core
    x, y, z = lax.rem(me, nx), lax.rem(me // nx, ny), me // (nx * ny)
    gpb = 128 // size
    lanes = gpb * state
    blocks = groups // gpb
    chunks = 16
    length = rows // chunks
    half = rows // ntp
    tall, wide = fin_v.shape[0] // 2, fin_v.shape[1]
    span = ntp * tall
    lead = ntp - 1
    fold = lanes // wide
    per = 128 // state

    quarter = rows // 4
    moves = [(ls_h, ls_v), (lr_h, lr_v), (li_h, li_v)]
    moves += [(x_h.at[pl.ds(i * quarter, quarter)], x_v.at[pl.ds(i * quarter, quarter)]) for i in range(4)]
    moves += [(s.at[pl.ds(i * groups // 2, groups // 2)], d.at[pl.ds(i * groups // 2, groups // 2)])
              for s, d in ((br_h, br_v), (bi_h, bi_v)) for i in range(2)]
    moves += [(cr_h, cr_v), (ci_h, ci_v), (sk_h, sk_v), (vb_h, vb_v), (gb_h, gb_v)]
    copies = [pltpu.make_async_copy(s, d, in_sem.at[i]) for i, (s, d) in enumerate(moves)]
    for c in copies:
        c.start()
    depth = vw_h.shape[0]

    def place_of(who):
        return pl.ds(pl.multiple_of(who * depth, depth), depth)

    def rows_of(who):
        return pl.ds(pl.multiple_of(who * half, half), half)

    weights = (vw_h, gw_h)
    own_w = [pltpu.make_async_copy(s, w_v.at[i, place_of(core)], w_sem.at[i]) for i, s in enumerate(weights)]

    def across(i, src, dst):
        return pltpu.make_async_remote_copy(
            src_ref=src, dst_ref=dst, send_sem=d_send.at[i], recv_sem=d_got.at[i],
            device_id=(me, other_core), device_id_type=MESH)

    out_w = [across(i, s, w_v.at[i, place_of(core)]) for i, s in enumerate(weights)]
    got_w = [across(i, s, w_v.at[i, place_of(other_core)]) for i, s in enumerate(weights)]
    out_par, got_par = (across(2, par_v.at[i], par_v.at[i]) for i in (core, other_core))
    out_gain, got_gain = (across(3, gain_v.at[i], gain_v.at[i]) for i in (core, other_core))
    out_resp = across(4, resp_v.at[rows_of(other_core)], both_v.at[core])
    got_resp = across(4, resp_v.at[rows_of(other_core)], both_v.at[other_core])
    out_h = across(5, pass_v, h_v)

    barrier = pltpu.get_barrier_semaphore()

    def hello(device):
        pl.semaphore_signal(barrier, inc=1, device_id=device, device_id_type=MESH)

    def peer(at, count, stride, k):
        other = lax.rem(at + k, count)
        return other, me + (other - at) * stride

    hello((me, other_core))
    lines = ((x, nx, 1), (y, ny, nx), (z, nz, nx * ny))

    @pl.when(core == lead)
    def _():
        for k in range(1, nx):
            for i in range(ntp):
                hello((peer(*lines[0], k)[1], i))
        for k in range(1, ny):
            hello((peer(*lines[1], k)[1], lead))

        @pl.loop(z + 1, nz)
        def _(d):
            hello((peer(*lines[2], d - z)[1], lead))

    bmat_v[...] = jnp.zeros_like(bmat_v)
    pair_mask = [iota((size, 128), 1) // state == i for i in range(per)]

    def spread(value, g):
        return jnp.where(pair_mask[g % per], jnp.concatenate([value] * per, axis=1), 0.0)

    for c in copies[:3]:
        c.wait()
    eye = iota((groups, groups), 0) == iota((groups, groups), 1)
    step = jnp.exp(jnp.sum(jnp.where(eye, ls_v[...], 0.0), axis=1, keepdims=True))
    lam_r, lam_i = lr_v[...], li_v[...]
    mag = jnp.exp(lam_r * step)
    phase = lam_i * step
    t_r, t_i = mag * jnp.cos(phase), mag * jnp.sin(phase)
    den = lam_r * lam_r + lam_i * lam_i
    n_r = t_r - 1.0
    f_r = (n_r * lam_r + t_i * lam_i) / den
    f_i = (t_i * lam_r - n_r * lam_i) / den

    row8, lane8 = iota((gpb, 128), 0), iota((gpb, 128), 1)

    def hold(at, value):
        for b in range(blocks):
            dup = jnp.concatenate([value[b * gpb:(b + 1) * gpb]] * per, axis=1)
            for j in range(gpb // per):
                tile = jnp.sum(jnp.where(row8 == per * j + lane8 // state, dup, 0.0), axis=0, keepdims=True)
                flat = j * 128
                r, c = b * fold + flat // wide, flat % wide
                par_v[core, at, r:r + 1, c:c + 128] = tile

    hold(0, t_r)
    hold(1, t_i)
    hold(2, f_r)
    hold(3, f_i)

    q_r, q_i = par_v[core, 0], par_v[core, 1]
    squares = rows.bit_length() - 1
    for k in range(squares):
        q_r, q_i = cmul(q_r, q_i, q_r, q_i)
        par_v[core, 4 + 2 * k] = q_r
        par_v[core, 5 + 2 * k] = q_i

    def row(k, b, who=core):
        return [jnp.concatenate(
            [par_v[who, 2 * k + i, b * fold + u:b * fold + u + 1] for u in range(fold)], axis=1) for i in range(2)]

    def power(exponent, b, who=core):
        return row(0 if exponent == 1 else exponent.bit_length(), b, who)

    def pair(k):
        return [jnp.concatenate([par_v[i, 2 * k + j] for i in range(ntp)], axis=0) for j in range(2)]

    row_b = iota((8, lanes), 0)

    def eight(b, flip, who=core):
        count = 7 - row_b if flip else row_b
        v_r, v_i = jnp.ones((8, lanes), F32), jnp.zeros((8, lanes), F32)
        for k in range(3):
            bit = (count // (1 << k)) % 2 == 1
            s_r, s_i = power(1 << k, b, who)
            v_r, v_i = cmul(v_r, v_i, jnp.where(bit, s_r, 1.0), jnp.where(bit, s_i, 0.0))
        return v_r, v_i

    for c in copies[3:11]:
        c.wait()
    late = 1 + (half.bit_length() - 1)
    for g in range(groups):
        b, l = g // gpb, g % gpb
        at, cols = l * size, l // per * 128
        lane = slice(cols, cols + 128)
        b_r, b_i = spread(br_v[g], g), spread(bi_v[g], g)
        e_r, e_i = row(late, b)
        m_r, m_i = cmul(b_r, b_i, e_r[:, lane], e_i[:, lane])
        for base, v_r, v_i in ((0, m_r, m_i), (128, b_r, b_i)):
            bmat_v[b, base + at:base + at + size, cols:cols + 128] = v_r.astype(BF16)
            bmat_v[b, base + at:base + at + size, lanes + cols:lanes + cols + 128] = v_i.astype(BF16)

    for b in range(blocks):
        cols = slice(b * 128, (b + 1) * 128)
        both = jnp.concatenate([x_v[:half, cols], x_v[half:, cols]], axis=1)
        out = jnp.dot(both, bmat_v[b], preferred_element_type=F32)
        e_r, e_i = power(8, b)
        z_r, z_i = out[:8, :lanes], out[:8, lanes:]
        for k in range(1, half // 8):
            p_r, p_i = cmul(e_r, e_i, z_r, z_i)
            z_r, z_i = p_r + out[8 * k:8 * k + 8, :lanes], p_i + out[8 * k:8 * k + 8, lanes:]
        v_r, v_i = cmul(*eight(b, True), z_r, z_i)
        v_r, v_i = jnp.sum(v_r, axis=0, keepdims=True), jnp.sum(v_i, axis=0, keepdims=True)
        for u in range(fold):
            at, cols = b * fold + u, slice(u * wide, (u + 1) * wide)
            fin_v[at:at + 1] = v_r[:, cols]
            fin_v[tall + at:tall + at + 1] = v_i[:, cols]
    end_v[...] = fin_v[...].astype(BF16)

    def to_row(k):
        other, device = peer(*lines[0], k)
        return pltpu.make_async_remote_copy(
            src_ref=end_v, dst_ref=recv_x.at[x, core], send_sem=send_x.at[other], recv_sem=got_x.at[x, core],
            device_id=(device, lead), device_id_type=MESH)

    def along(stage, k):
        at = lines[stage][0]
        other, device = peer(*lines[stage], k)
        message, recv, sent, got = ((), (row_v, recv_y, send_y, got_y), (plane_v, recv_z, send_z, got_z))[stage]
        return pltpu.make_async_remote_copy(
            src_ref=message, dst_ref=recv.at[at], send_sem=sent.at[other], recv_sem=got.at[at],
            device_id=(device, lead), device_id_type=MESH)

    def arrived(recv, got, sent, at, device):
        pltpu.make_async_remote_copy(
            src_ref=recv.at[at], dst_ref=recv.at[at], send_sem=sent, recv_sem=got.at[at],
            device_id=device, device_id_type=MESH).wait_recv()

    def from_row(k):
        other, device = peer(*lines[0], k)
        parts = []
        for i in range(ntp):
            if k == 0 and i == lead:
                parts.append(fin_v[...])
                continue
            arrived(recv_x, got_x, send_x.at[other], (other, i), (device, i))
            parts.append(recv_x[other, i].astype(F32))
        return (other, jnp.concatenate([p[:tall] for p in parts], axis=0),
                jnp.concatenate([p[tall:] for p in parts], axis=0))

    def from_line(stage, k):
        other, device = peer(*lines[stage], k)
        recv, sent, got = ((), (recv_y, send_y, got_y), (recv_z, send_z, got_z))[stage]
        arrived(recv, got, sent.at[other], other, (device, lead))
        value = recv[other].astype(F32)
        return other, value[:span], value[span:]

    @pl.when(core == lead)
    def _():
        pl.semaphore_wait(barrier, nx - 1 + ny - 1 + ntp - 1 + z)
        for k in reversed(near_first(nx)):
            to_row(k).start()

        @pl.loop(0, z)
        def _(d):
            pl.semaphore_signal(
                ready.at[z], inc=1, device_id=(peer(*lines[2], d - z + nz)[1], lead), device_id_type=MESH)

    @pl.when(core != lead)
    def _():
        pl.semaphore_wait(barrier, nx - 1 + ntp - 1)
        for k in list(reversed(near_first(nx))) + [0]:
            to_row(k).start()

    out_par.start()
    for c in own_w:
        c.start()

    mats_v[...] = jnp.zeros_like(mats_v)
    keep_v[...] = jnp.zeros_like(keep_v)
    for c in copies[11:14]:
        c.wait()

    def place(ref, b, l, v_r, v_i):
        at, cols = l * size, l // per * 128
        ref[b, at:at + size, cols:cols + 128] = v_r.astype(BF16)
        ref[b, at:at + size, lanes + cols:lanes + cols + 128] = (-v_i).astype(BF16)

    for g in range(groups):
        b, l = g // gpb, g % gpb
        f_r, f_i = row(1, b)
        cols = slice(l // per * 128, l // per * 128 + 128)
        c_r, c_i = cmul(spread(cr_v[g], g), spread(ci_v[g], g), f_r[:, cols], f_i[:, cols])
        gain_v[core, 0, g], gain_v[core, 1, g] = c_r, c_i
        place(mats_v, b, l, c_r, c_i)
    out_gain.start()
    for c in out_w:
        c.start()

    r0, r1 = iota((rows, rows), 0), iota((rows, rows), 1)
    shuffle = jnp.where(r1 == (r0 % chunks) * length + r0 // chunks, 1.0, 0.0).astype(BF16)
    back = jnp.where(r1 == (r0 % length) * chunks + r0 // length, 1.0, 0.0).astype(BF16)
    xp_v[...] = jnp.dot(shuffle, x_v[...], preferred_element_type=F32).astype(BF16)
    crow = iota((chunks, lanes), 0)

    def shift(value, s):
        return jnp.where(crow >= s, pltpu.roll(value, s, 0), 0.0)

    def respond(b):
        out = jnp.dot(xp_v[:, b * 128:(b + 1) * 128], bmat_v[b, 128:], preferred_element_type=F32)
        zr_v[b] = out[:, :lanes]
        zi_v[b] = out[:, lanes:]
        a_r, a_i = power(1, b)
        z_r, z_i = zr_v[b, :chunks, :], zi_v[b, :chunks, :]
        for o in range(1, length):
            here = pl.ds(o * chunks, chunks)
            p_r, p_i = cmul(a_r, a_i, z_r, z_i)
            z_r, z_i = p_r + zr_v[b, here, :], p_i + zi_v[b, here, :]
            zr_v[b, here, :] = z_r
            zi_v[b, here, :] = z_i
        s = 1
        while s < chunks:
            m_r, m_i = cmul(*power(length * s, b), shift(z_r, s), shift(z_i, s))
            z_r, z_i = z_r + m_r, z_i + m_i
            s *= 2
        w_r, w_i = shift(z_r, 1), shift(z_i, 1)
        for o in range(length):
            here = pl.ds(o * chunks, chunks)
            w_r, w_i = cmul(a_r, a_i, w_r, w_i)
            zcat_v[b, here, :lanes] = (zr_v[b, here, :] + w_r).astype(BF16)
            zcat_v[b, here, lanes:] = (zi_v[b, here, :] + w_i).astype(BF16)
        col = pl.ds(b * 128, 128)
        out = nt_dot(zcat_v[b], mats_v[b])
        high = out.astype(BF16)
        low = (out - high.astype(F32)).astype(BF16)
        turned = jnp.dot(back, jnp.concatenate([high, low], axis=1), preferred_element_type=F32)
        resp_v[:, col] = turned[:, :128] + turned[:, 128:] + sk_v[:, col] * x_v[:, col].astype(F32)

    def carry_powers(i, which):
        each = [(b, power(8, b, i)) for b in which]
        value = [cmul(*power(1, b, i), *eight(b, False, i)) for b in which]
        for o in range(half // 16):
            here = pl.ds(o * 16, 16)
            after = [cmul(*e, *v) for (_, e), v in zip(each, value)]
            for (b, _), v, n in zip(each, value, after):
                wcat_v[i, b, here, :lanes] = jnp.concatenate([v[0], n[0]], axis=0).astype(BF16)
                wcat_v[i, b, here, lanes:] = jnp.concatenate([v[1], n[1]], axis=0).astype(BF16)
            value = [cmul(*e, *n) for (_, e), n in zip(each, after)]

    def powers(tab, count, a_r, a_i):
        p_r, p_i = jnp.ones((span, wide), F32), jnp.zeros((span, wide), F32)
        for i in range(count):
            tab[i] = jnp.zeros((2 * span, wide), F32)
            tab[count + i, :span], tab[count + i, span:] = p_r, p_i
            p_r, p_i = cmul(p_r, p_i, a_r, a_i)
        return p_r, p_i

    def weight(tab, at, v_r, v_i):
        return cmul(tab[at, :span], tab[at, span:], v_r, v_i)

    def collect(stage, tab, own_r, own_i, receive):
        at, count, _ = lines[stage]
        t_r, t_i = weight(tab, count + count - 1 - at, own_r, own_i)
        p_r = p_i = jnp.zeros((span, wide), F32)
        for k in near_first(count):
            other, v_r, v_i = receive(k)
            m_r, m_i = weight(tab, count + count - 1 - other, v_r, v_i)
            t_r, t_i = t_r + m_r, t_i + m_i
            m_r, m_i = weight(tab, count + at - 1 - other, v_r, v_i)
            p_r, p_i = p_r + m_r, p_i + m_i
        return t_r, t_i, p_r, p_i

    respond(0)
    got_par.wait_recv()

    @pl.when(core == lead)
    def _():
        ax_r, ax_i = powers(tab_x, nx, *pair(1 + squares))
        ay_r, ay_i = powers(tab_y, ny, ax_r, ax_i)
        sum_v[4], sum_v[5] = ay_r, ay_i
        _, own_r, own_i = from_row(0)
        t_r, t_i, p_r, p_i = collect(0, tab_x, own_r, own_i, from_row)
        row_v[:span], row_v[span:] = t_r.astype(BF16), t_i.astype(BF16)
        for k in reversed(near_first(ny)):
            along(1, k).start()
        sum_v[0], sum_v[1], sum_v[2], sum_v[3] = t_r, t_i, p_r, p_i

    for b in range(1, blocks - 1):
        respond(b)
    for b in range(0, blocks, 2):
        carry_powers(core, (b, b + 1))

    @pl.when(core == lead)
    def _():
        t_r, t_i, y_r, y_i = collect(1, tab_y, sum_v[0], sum_v[1], functools.partial(from_line, 1))
        plane_v[:span], plane_v[span:] = t_r.astype(BF16), t_i.astype(BF16)

        @pl.loop(z + 1, nz)
        def _(d):
            pl.semaphore_wait(ready.at[d], 1)
            along(2, d - z).start()

        m_r, m_i = weight(tab_x, nx + x, y_r, y_i)
        sum_v[2], sum_v[3] = sum_v[2] + m_r, sum_v[3] + m_i
        sum_v[0], sum_v[1] = weight(tab_x, nx + x, tab_y[ny + y, :span], tab_y[ny + y, span:])

    respond(blocks - 1)
    out_resp.start()
    both_v[core] = resp_v[rows_of(core), :]
    for b in range(0, blocks, 2):
        carry_powers(other_core, (b, b + 1))

    @pl.when(core == lead)
    def _():
        def gather(k, carry):
            h_r, h_i, p_r, p_i = carry
            _, v_r, v_i = from_line(2, nz - 1 - k)
            m_r, m_i = cmul(p_r, p_i, v_r, v_i)
            return (h_r + m_r, h_i + m_i) + cmul(p_r, p_i, sum_v[4], sum_v[5])

        h_r, h_i, _, _ = lax.fori_loop(0, z, gather, (sum_v[2], sum_v[3], sum_v[0], sum_v[1]))
        pass_v[:span], pass_v[span:] = h_r, h_i
        out_h.start()
        h_v[:span], h_v[span:] = cmul(*pair(late), h_r, h_i)

    @pl.when(core != lead)
    def _():
        out_h.wait_recv()

    got_gain.wait_recv()
    got_resp.wait_recv()
    for i in range(ntp):
        for b in range(blocks):
            for l in range(gpb):
                g, flat = b * gpb + l, l // per * 128
                r, cols = i * tall + b * fold + flat // wide, slice(flat % wide, flat % wide + 128)
                place(keep_v.at[i], b, l, *cmul(
                    gain_v[i, 0, g], gain_v[i, 1, g], h_v[r:r + 1, cols], h_v[span + r:span + r + 1, cols]))
            col = pl.ds(b * 128, 128)
            total = nt_dot(wcat_v[i, b], keep_v[i, b]) + both_v[i, :, col]
            act_v[:, pl.ds(i * depth + b * 128, 128)] = jax.nn.gelu(total).astype(BF16)
    for c in copies[14:]:
        c.wait()
    for c in own_w:
        c.wait()
    for c in got_w:
        c.wait_recv()
    piece = min(512, width)
    for col in [pl.ds(j * piece, piece) for j in range(width // piece)]:
        sums = [bias[:, col] + jnp.dot(act_v[...], w_v[i, :, col], preferred_element_type=F32)
                for i, bias in enumerate((vb_v, gb_v))]
        out_ref[:, col] = (sums[0] * jax.nn.sigmoid(sums[1])).astype(BF16)
    for c in out_w + [out_par, out_gain, out_resp]:
        c.wait_send()
    for k in range(1, nx):
        to_row(k).wait_send()

    @pl.when(core == lead)
    def _():
        out_h.wait_send()
        for k in range(1, ny):
            along(1, k).wait_send()

        @pl.loop(z + 1, nz)
        def _(d):
            along(2, d - z).wait_send()

    @pl.when(core != lead)
    def _():
        to_row(0).wait_send()


def local(nsp, ntp, features, lambda_real, lambda_imag, log_step, input_real, input_imag, real_output,
          imaginary_output, skip_gain, value_weight, gate_weight, value_bias, gate_bias):
    rows, channels = features.shape
    groups, state = lambda_real.shape
    size = input_real.shape[2]
    input_real, input_imag = jnp.swapaxes(input_real, 1, 2), jnp.swapaxes(input_imag, 1, 2)
    width = value_weight.shape[1]
    gpb = 128 // size
    lanes, blocks = gpb * state, groups // gpb
    ring = nz, ny, nx = split_ring(nsp)
    held = (16, 2 * blocks * lanes // 16)
    pairs = (ntp * held[0], held[1])
    half = rows // ntp
    args = (features, lambda_real, lambda_imag, log_step[None], input_real, input_imag, real_output,
            imaginary_output, skip_gain[None], value_weight, gate_weight, value_bias[None], gate_bias[None])
    scratch = [pltpu.VMEM(a.shape, a.dtype) for a in args[:9] + args[11:]]
    scratch += [
        pltpu.VMEM((2, ntp * channels, width), BF16),
        pltpu.VMEM((rows, channels), BF16),
        pltpu.VMEM((blocks, 256, 2 * lanes), BF16),
        pltpu.VMEM((blocks, 128, 2 * lanes), BF16),
        pltpu.VMEM((ntp, blocks, 128, 2 * lanes), BF16),
        pltpu.VMEM((blocks, rows, lanes), F32),
        pltpu.VMEM((blocks, rows, lanes), F32),
        pltpu.VMEM((blocks, rows, 2 * lanes), BF16),
        pltpu.VMEM((ntp, blocks, half, 2 * lanes), BF16),
        pltpu.VMEM((ntp, 2, groups, size, 128), F32),
        pltpu.VMEM((rows, channels), F32),
        pltpu.VMEM((ntp, half, channels), F32),
        pltpu.VMEM((half, ntp * channels), BF16),
        pltpu.VMEM((ntp, 4 + 2 * (rows.bit_length() - 1), 8, held[1]), F32),
        pltpu.VMEM(held, F32),
        pltpu.VMEM((2 * nx,) + pairs, F32),
        pltpu.VMEM((2 * ny,) + pairs, F32),
        pltpu.VMEM((6, pairs[0] // 2, pairs[1]), F32),
        pltpu.VMEM(held, BF16),
        pltpu.VMEM(pairs, BF16),
        pltpu.VMEM(pairs, BF16),
        pltpu.VMEM((nx, ntp) + held, BF16),
        pltpu.VMEM((ny,) + pairs, BF16),
        pltpu.VMEM((nz,) + pairs, BF16),
        pltpu.VMEM(pairs, F32),
        pltpu.VMEM(pairs, F32),
        pltpu.SemaphoreType.DMA((16,)),
        pltpu.SemaphoreType.DMA((2,)),
        pltpu.SemaphoreType.DMA((nx,)),
        pltpu.SemaphoreType.DMA((nx, ntp)),
        pltpu.SemaphoreType.DMA((ny,)),
        pltpu.SemaphoreType.DMA((ny,)),
        pltpu.SemaphoreType.DMA((nz,)),
        pltpu.SemaphoreType.DMA((nz,)),
        pltpu.SemaphoreType.REGULAR((nz,)),
        pltpu.SemaphoreType.DMA((6,)),
        pltpu.SemaphoreType.DMA((6,)),
    ]
    return pl.pallas_call(
        functools.partial(kernel, ring, ntp, (rows, groups, state, size, width)),
        out_shape=pltpu.VMEM((rows // ntp, width), BF16),
        in_specs=[pl.BlockSpec(memory_space=pl.ANY)] * len(args),
        out_specs=pl.BlockSpec(memory_space=pltpu.VMEM),
        scratch_shapes=scratch,
        compiler_params=pltpu.CompilerParams(
            collective_id=0, has_side_effects=True, vmem_limit_bytes=60 * 1024 * 1024),
        name="mixer",
    )(*args)


def solution(mesh):
    in_specs = (
        P("sp", "tp"),
        P("tp", None),
        P("tp", None),
        P("tp"),
        P("tp", None, None),
        P("tp", None, None),
        P("tp", None, None),
        P("tp", None, None),
        P("tp"),
        P("tp", None),
        P("tp", None),
        P(),
        P(),
    )
    out_specs = P(("sp", "tp"), None)
    body = functools.partial(local, mesh.shape["sp"], mesh.shape["tp"])
    return jax.shard_map(body, mesh=mesh, in_specs=in_specs, out_specs=out_specs, check_vma=False)
```

time: 22.5 us -> 21.8 us (0.969); the launches traced: 22.1 us -> 21.7 us
  Pallas kernels: 21.3 us -> 20.9 us
    pallas_call x1, Pallas kernels: 21.3 us -> 20.9 us  [local(): pl.pallas_call(functools.partial(kernel, ring, ntp, (rows, groups, state,...]
where the time goes in v4:
time: 21.8 us; the launch traced here: 21.7 us
  Pallas kernels  20.9 us (96%)
  local copies, waits for them, and re-layouts  0.8 us (4%)
    pallas_call x1, Pallas kernels, local(): pl.pallas_call(functools.partial(kernel, ring, ntp, (rows, groups, state,...  20.9 us
    unnamed x1, local copies, waits for them, and re-layouts  0.8 us

profile of v4, /device:TPU:1, one launch (start us, length us, event | category | flops | bytes accessed | tf_op | source)
XLA Modules:
  0.0 21.7 jit_solution(8408444781911394801)
XLA Ops:
  0.0 20.9 %mixer.1 = bf16[128,2048]{1,0:T(8,128)(2,1)S(1)} custom-call(bf16[256,512]{1,0:T(8,128)(2,1)} %refs_0_.1, f32[32,64]{1,0:T(8,128)} %refs_1_.1, f32[32,64]{1,0:T(8,128)} %refs_2_.1, f32[1,32]{1,0:T(1,128)} %bitcast.11, f32[32,16,64]{2,1,0:T(8,128)} %bitcast.6, f32[32,16,64]{2,1,0:T(8,128)} %bitcast.7, f32[32,16,64]{2,1,0:T(8,128)} %refs_6_.1, ...), custom_call_target="tpu_custom_call" | custom-call | tf_op jit(solution)/shard_map/mixer/pallas_call | solution.py:520
  20.9 0.8 %copy.15 = bf16[128,2048]{1,0:T(8,128)(2,1)} copy(bf16[128,2048]{1,0:T(8,128)(2,1)S(1)} %mixer.1) | data formatting | bytes 1048576

commit v5 on v4

--- a/solution.py
+++ b/solution.py
@@ -38,10 +38,10 @@
     nz, ny, nx = ring
     rows, groups, state, size, width = dims
     (x_h, lr_h, li_h, ls_h, br_h, bi_h, cr_h, ci_h, sk_h, vw_h, gw_h, vb_h, gb_h, out_ref,
-     x_v, lr_v, li_v, ls_v, br_v, bi_v, cr_v, ci_v, sk_v, vb_v, gb_v, w_v,
+     x_v, ls_v, lam_v, b_v, c_v, sk_v, bias_v, w_v,
      xp_v, bmat_v, mats_v, keep_v, zr_v, zi_v, zcat_v, wcat_v, gain_v, resp_v, both_v, act_v,
      par_v, fin_v, tab_x, tab_y, sum_v, end_v, row_v, plane_v, recv_x, recv_y, recv_z, h_v, pass_v,
-     in_sem, w_sem, send_x, got_x, send_y, got_y, send_z, got_z, ready, d_send, d_got) = refs
+     sems, got_sems, ready) = refs
     me = lax.axis_index("sp")
     core = lax.axis_index("tp")
     other_core = 1 - core
@@ -58,15 +58,19 @@
     fold = lanes // wide
     per = 128 // state
 
+    (s_step, s_lam, s_x, s_b, s_c, s_skip, s_bias, s_w, s_h) = (sems.at[i] for i in range(9))
+    (g_x, g_y, g_z, g_par, g_gain, g_resp, g_h, g_w0, g_w1) = (got_sems.at[i] for i in range(9))
+
+    def settle(ref, sem):
+        pltpu.make_async_copy(ref, ref, sem).wait()
+
     quarter = rows // 4
-    moves = [(ls_h, ls_v), (lr_h, lr_v), (li_h, li_v)]
-    moves += [(x_h.at[pl.ds(i * quarter, quarter)], x_v.at[pl.ds(i * quarter, quarter)]) for i in range(4)]
-    moves += [(s.at[pl.ds(i * groups // 2, groups // 2)], d.at[pl.ds(i * groups // 2, groups // 2)])
-              for s, d in ((br_h, br_v), (bi_h, bi_v)) for i in range(2)]
-    moves += [(cr_h, cr_v), (ci_h, ci_v), (sk_h, sk_v), (vb_h, vb_v), (gb_h, gb_v)]
-    copies = [pltpu.make_async_copy(s, d, in_sem.at[i]) for i, (s, d) in enumerate(moves)]
-    for c in copies:
-        c.start()
+    moves = [(ls_h, ls_v, s_step), (lr_h, lam_v.at[0], s_lam), (li_h, lam_v.at[1], s_lam)]
+    moves += [(x_h.at[pl.ds(i * quarter, quarter)], x_v.at[pl.ds(i * quarter, quarter)], s_x) for i in range(4)]
+    moves += [(br_h, b_v.at[0], s_b), (bi_h, b_v.at[1], s_b), (cr_h, c_v.at[0], s_c), (ci_h, c_v.at[1], s_c)]
+    moves += [(sk_h, sk_v, s_skip), (vb_h, bias_v.at[0], s_bias), (gb_h, bias_v.at[1], s_bias)]
+    for src, dst, sem in moves:
+        pltpu.make_async_copy(src, dst, sem).start()
     depth = vw_h.shape[0]
 
     def place_of(who):
@@ -76,20 +80,20 @@
         return pl.ds(pl.multiple_of(who * half, half), half)
 
     weights = (vw_h, gw_h)
-    own_w = [pltpu.make_async_copy(s, w_v.at[i, place_of(core)], w_sem.at[i]) for i, s in enumerate(weights)]
-
-    def across(i, src, dst):
+
+    def across(src, dst, sent, got):
         return pltpu.make_async_remote_copy(
-            src_ref=src, dst_ref=dst, send_sem=d_send.at[i], recv_sem=d_got.at[i],
+            src_ref=src, dst_ref=dst, send_sem=sent, recv_sem=got,
             device_id=(me, other_core), device_id_type=MESH)
 
-    out_w = [across(i, s, w_v.at[i, place_of(core)]) for i, s in enumerate(weights)]
-    got_w = [across(i, s, w_v.at[i, place_of(other_core)]) for i, s in enumerate(weights)]
-    out_par, got_par = (across(2, par_v.at[i], par_v.at[i]) for i in (core, other_core))
-    out_gain, got_gain = (across(3, gain_v.at[i], gain_v.at[i]) for i in (core, other_core))
-    out_resp = across(4, resp_v.at[rows_of(other_core)], both_v.at[core])
-    got_resp = across(4, resp_v.at[rows_of(other_core)], both_v.at[other_core])
-    out_h = across(5, pass_v, h_v)
+    wcols = [pl.ds(i * (width // 2), width // 2) for i in range(2)]
+    out_w = [[across(s.at[:, cols], w_v.at[i, place_of(core), cols], s_c, got) for i, s in enumerate(weights)]
+             for cols, got in zip(wcols, (g_w0, g_w1))]
+    out_par, got_par = (across(par_v.at[i], par_v.at[i], s_lam, g_par) for i in (core, other_core))
+    out_gain, got_gain = (across(gain_v.at[i], gain_v.at[i], s_b, g_gain) for i in (core, other_core))
+    out_resp = across(resp_v.at[rows_of(other_core)], both_v.at[core], s_bias, g_resp)
+    got_resp = across(resp_v.at[rows_of(other_core)], both_v.at[other_core], s_bias, g_resp)
+    out_h = across(pass_v, h_v, s_h, g_h)
 
     barrier = pltpu.get_barrier_semaphore()
 
@@ -121,11 +125,11 @@
     def spread(value, g):
         return jnp.where(pair_mask[g % per], jnp.concatenate([value] * per, axis=1), 0.0)
 
-    for c in copies[:3]:
-        c.wait()
+    settle(ls_v, s_step)
+    settle(lam_v, s_lam)
     eye = iota((groups, groups), 0) == iota((groups, groups), 1)
     step = jnp.exp(jnp.sum(jnp.where(eye, ls_v[...], 0.0), axis=1, keepdims=True))
-    lam_r, lam_i = lr_v[...], li_v[...]
+    lam_r, lam_i = lam_v[0], lam_v[1]
     mag = jnp.exp(lam_r * step)
     phase = lam_i * step
     t_r, t_i = mag * jnp.cos(phase), mag * jnp.sin(phase)
@@ -178,14 +182,14 @@
             v_r, v_i = cmul(v_r, v_i, jnp.where(bit, s_r, 1.0), jnp.where(bit, s_i, 0.0))
         return v_r, v_i
 
-    for c in copies[3:11]:
-        c.wait()
+    settle(x_v, s_x)
+    settle(b_v, s_b)
     late = 1 + (half.bit_length() - 1)
     for g in range(groups):
         b, l = g // gpb, g % gpb
         at, cols = l * size, l // per * 128
         lane = slice(cols, cols + 128)
-        b_r, b_i = spread(br_v[g], g), spread(bi_v[g], g)
+        b_r, b_i = spread(b_v[0, g], g), spread(b_v[1, g], g)
         e_r, e_i = row(late, b)
         m_r, m_i = cmul(b_r, b_i, e_r[:, lane], e_i[:, lane])
         for base, v_r, v_i in ((0, m_r, m_i), (128, b_r, b_i)):
@@ -212,39 +216,32 @@
     def to_row(k):
         other, device = peer(*lines[0], k)
         return pltpu.make_async_remote_copy(
-            src_ref=end_v, dst_ref=recv_x.at[x, core], send_sem=send_x.at[other], recv_sem=got_x.at[x, core],
+            src_ref=end_v, dst_ref=recv_x.at[x * ntp + core], send_sem=s_step, recv_sem=g_x,
             device_id=(device, lead), device_id_type=MESH)
 
     def along(stage, k):
         at = lines[stage][0]
         other, device = peer(*lines[stage], k)
-        message, recv, sent, got = ((), (row_v, recv_y, send_y, got_y), (plane_v, recv_z, send_z, got_z))[stage]
+        message, recv, sent, got = ((), (row_v, recv_y, s_x, g_y), (plane_v, recv_z, s_skip, g_z))[stage]
         return pltpu.make_async_remote_copy(
-            src_ref=message, dst_ref=recv.at[at], send_sem=sent.at[other], recv_sem=got.at[at],
+            src_ref=message, dst_ref=recv.at[at], send_sem=sent, recv_sem=got,
             device_id=(device, lead), device_id_type=MESH)
 
-    def arrived(recv, got, sent, at, device):
-        pltpu.make_async_remote_copy(
-            src_ref=recv.at[at], dst_ref=recv.at[at], send_sem=sent, recv_sem=got.at[at],
-            device_id=device, device_id_type=MESH).wait_recv()
+    def settle_some(ref, sem, count, most):
+        for i in range(1, most):
+            @pl.when(count == i)
+            def _():
+                settle(ref.at[pl.ds(0, i)], sem)
 
     def from_row(k):
         other, device = peer(*lines[0], k)
-        parts = []
-        for i in range(ntp):
-            if k == 0 and i == lead:
-                parts.append(fin_v[...])
-                continue
-            arrived(recv_x, got_x, send_x.at[other], (other, i), (device, i))
-            parts.append(recv_x[other, i].astype(F32))
+        parts = [fin_v[...] if k == 0 and i == lead else recv_x[other * ntp + i].astype(F32) for i in range(ntp)]
         return (other, jnp.concatenate([p[:tall] for p in parts], axis=0),
                 jnp.concatenate([p[tall:] for p in parts], axis=0))
 
     def from_line(stage, k):
         other, device = peer(*lines[stage], k)
-        recv, sent, got = ((), (recv_y, send_y, got_y), (recv_z, send_z, got_z))[stage]
-        arrived(recv, got, sent.at[other], other, (device, lead))
-        value = recv[other].astype(F32)
+        value = ((), recv_y, recv_z)[stage][other].astype(F32)
         return other, value[:span], value[span:]
 
     @pl.when(core == lead)
@@ -265,13 +262,14 @@
             to_row(k).start()
 
     out_par.start()
-    for c in own_w:
-        c.start()
+    for i, s in enumerate(weights):
+        pltpu.make_async_copy(s, w_v.at[i, place_of(core)], s_w).start()
 
     mats_v[...] = jnp.zeros_like(mats_v)
     keep_v[...] = jnp.zeros_like(keep_v)
-    for c in copies[11:14]:
-        c.wait()
+    settle(c_v, s_c)
+    settle(sk_v, s_skip)
+    settle(bias_v, s_bias)
 
     def place(ref, b, l, v_r, v_i):
         at, cols = l * size, l // per * 128
@@ -282,12 +280,17 @@
         b, l = g // gpb, g % gpb
         f_r, f_i = row(1, b)
         cols = slice(l // per * 128, l // per * 128 + 128)
-        c_r, c_i = cmul(spread(cr_v[g], g), spread(ci_v[g], g), f_r[:, cols], f_i[:, cols])
+        c_r, c_i = cmul(spread(c_v[0, g], g), spread(c_v[1, g], g), f_r[:, cols], f_i[:, cols])
         gain_v[core, 0, g], gain_v[core, 1, g] = c_r, c_i
         place(mats_v, b, l, c_r, c_i)
     out_gain.start()
-    for c in out_w:
+    for c in out_w[0]:
         c.start()
+
+    @pl.when(core == lead)
+    def _():
+        for c in out_w[1]:
+            c.start()
 
     r0, r1 = iota((rows, rows), 0), iota((rows, rows), 1)
     shuffle = jnp.where(r1 == (r0 % chunks) * length + r0 // chunks, 1.0, 0.0).astype(BF16)
@@ -370,6 +373,7 @@
         ax_r, ax_i = powers(tab_x, nx, *pair(1 + squares))
         ay_r, ay_i = powers(tab_y, ny, ax_r, ax_i)
         sum_v[4], sum_v[5] = ay_r, ay_i
+        settle(recv_x.at[pl.ds(0, nx * ntp - 1)], g_x)
         _, own_r, own_i = from_row(0)
         t_r, t_i, p_r, p_i = collect(0, tab_x, own_r, own_i, from_row)
         row_v[:span], row_v[span:] = t_r.astype(BF16), t_i.astype(BF16)
@@ -384,6 +388,7 @@
 
     @pl.when(core == lead)
     def _():
+        settle(recv_y.at[pl.ds(0, ny - 1)], g_y)
         t_r, t_i, y_r, y_i = collect(1, tab_y, sum_v[0], sum_v[1], functools.partial(from_line, 1))
         plane_v[:span], plane_v[span:] = t_r.astype(BF16), t_i.astype(BF16)
 
@@ -396,14 +401,31 @@
         sum_v[2], sum_v[3] = sum_v[2] + m_r, sum_v[3] + m_i
         sum_v[0], sum_v[1] = weight(tab_x, nx + x, tab_y[ny + y, :span], tab_y[ny + y, span:])
 
+    def hand_on(h_r, h_i):
+        pass_v[:span], pass_v[span:] = h_r, h_i
+        out_h.start()
+        h_v[:span], h_v[span:] = cmul(*pair(late), h_r, h_i)
+
+    @pl.when((core == lead) & (z == 0))
+    def _():
+        hand_on(sum_v[2], sum_v[3])
+
     respond(blocks - 1)
     out_resp.start()
+
+    @pl.when(core != lead)
+    def _():
+        for c in out_w[1]:
+            c.start()
+
     both_v[core] = resp_v[rows_of(core), :]
     for b in range(0, blocks, 2):
         carry_powers(other_core, (b, b + 1))
 
-    @pl.when(core == lead)
-    def _():
+    @pl.when((core == lead) & (z > 0))
+    def _():
+        settle_some(recv_z, g_z, z, nz)
+
         def gather(k, carry):
             h_r, h_i, p_r, p_i = carry
             _, v_r, v_i = from_line(2, nz - 1 - k)
@@ -411,9 +433,7 @@
             return (h_r + m_r, h_i + m_i) + cmul(p_r, p_i, sum_v[4], sum_v[5])
 
         h_r, h_i, _, _ = lax.fori_loop(0, z, gather, (sum_v[2], sum_v[3], sum_v[0], sum_v[1]))
-        pass_v[:span], pass_v[span:] = h_r, h_i
-        out_h.start()
-        h_v[:span], h_v[span:] = cmul(*pair(late), h_r, h_i)
+        hand_on(h_r, h_i)
 
     @pl.when(core != lead)
     def _():
@@ -431,35 +451,29 @@
             col = pl.ds(b * 128, 128)
             total = nt_dot(wcat_v[i, b], keep_v[i, b]) + both_v[i, :, col]
             act_v[:, pl.ds(i * depth + b * 128, 128)] = jax.nn.gelu(total).astype(BF16)
-    for c in copies[14:]:
-        c.wait()
-    for c in own_w:
-        c.wait()
-    for c in got_w:
-        c.wait_recv()
+    settle(w_v.at[:, place_of(core)], s_w)
+    settle(w_v.at[:, place_of(other_core), wcols[0]], g_w0)
     piece = min(512, width)
-    for col in [pl.ds(j * piece, piece) for j in range(width // piece)]:
-        sums = [bias[:, col] + jnp.dot(act_v[...], w_v[i, :, col], preferred_element_type=F32)
-                for i, bias in enumerate((vb_v, gb_v))]
+    for j in range(width // piece):
+        col = pl.ds(j * piece, piece)
+        if j * piece == width // 2:
+            settle(w_v.at[:, place_of(other_core), wcols[1]], g_w1)
+        sums = [bias_v[i, :, col] + jnp.dot(act_v[...], w_v[i, :, col], preferred_element_type=F32) for i in range(2)]
         out_ref[:, col] = (sums[0] * jax.nn.sigmoid(sums[1])).astype(BF16)
-    for c in out_w + [out_par, out_gain, out_resp]:
+    settle(w_v.at[:, place_of(core)], s_c)
+    for c in (out_par, out_gain, out_resp):
         c.wait_send()
-    for k in range(1, nx):
-        to_row(k).wait_send()
 
     @pl.when(core == lead)
     def _():
+        settle(recv_x.at[pl.ds(0, nx - 1)], s_step)
         out_h.wait_send()
-        for k in range(1, ny):
-            along(1, k).wait_send()
-
-        @pl.loop(z + 1, nz)
-        def _(d):
-            along(2, d - z).wait_send()
+        settle(recv_y.at[pl.ds(0, ny - 1)], s_x)
+        settle_some(recv_z, s_skip, nz - 1 - z, nz)
 
     @pl.when(core != lead)
     def _():
-        to_row(0).wait_send()
+        settle(recv_x.at[pl.ds(0, nx)], s_step)
 
 
 def local(nsp, ntp, features, lambda_real, lambda_imag, log_step, input_real, input_imag, real_output,
@@ -477,7 +491,15 @@
     half = rows // ntp
     args = (features, lambda_real, lambda_imag, log_step[None], input_real, input_imag, real_output,
             imaginary_output, skip_gain[None], value_weight, gate_weight, value_bias[None], gate_bias[None])
-    scratch = [pltpu.VMEM(a.shape, a.dtype) for a in args[:9] + args[11:]]
+    scratch = [
+        pltpu.VMEM(features.shape, BF16),
+        pltpu.VMEM((1, groups), F32),
+        pltpu.VMEM((2, groups, state), F32),
+        pltpu.VMEM((2, groups, size, state), F32),
+        pltpu.VMEM((2, groups, size, state), F32),
+        pltpu.VMEM((1, channels), F32),
+        pltpu.VMEM((2, 1, width), F32),
+    ]
     scratch += [
         pltpu.VMEM((2, ntp * channels, width), BF16),
         pltpu.VMEM((rows, channels), BF16),
@@ -500,22 +522,14 @@
         pltpu.VMEM(held, BF16),
         pltpu.VMEM(pairs, BF16),
         pltpu.VMEM(pairs, BF16),
-        pltpu.VMEM((nx, ntp) + held, BF16),
+        pltpu.VMEM((nx * ntp,) + held, BF16),
         pltpu.VMEM((ny,) + pairs, BF16),
         pltpu.VMEM((nz,) + pairs, BF16),
         pltpu.VMEM(pairs, F32),
         pltpu.VMEM(pairs, F32),
-        pltpu.SemaphoreType.DMA((16,)),
-        pltpu.SemaphoreType.DMA((2,)),
-        pltpu.SemaphoreType.DMA((nx,)),
-        pltpu.SemaphoreType.DMA((nx, ntp)),
-        pltpu.SemaphoreType.DMA((ny,)),
-        pltpu.SemaphoreType.DMA((ny,)),
-        pltpu.SemaphoreType.DMA((nz,)),
-        pltpu.SemaphoreType.DMA((nz,)),
+        pltpu.SemaphoreType.DMA((9,)),
+        pltpu.SemaphoreType.DMA((9,)),
         pltpu.SemaphoreType.REGULAR((nz,)),
-        pltpu.SemaphoreType.DMA((6,)),
-        pltpu.SemaphoreType.DMA((6,)),
     ]
     return pl.pallas_call(
         functools.partial(kernel, ring, ntp, (rows, groups, state, size, width)),

time: 21.8 us -> 20.9 us (0.959)
  Pallas kernels: 20.9 us -> 20 us
    pallas_call x1, Pallas kernels: 20.9 us -> 20 us  [local(): pl.pallas_call(functools.partial(kernel, ring, ntp, (rows, groups, state,...]
where the time goes in v5:
time: 20.9 us; the launch traced here: 20.8 us
  Pallas kernels  20 us (96%)
  local copies, waits for them, and re-layouts  0.8 us (4%)
    pallas_call x1, Pallas kernels, local(): pl.pallas_call(functools.partial(kernel, ring, ntp, (rows, groups, state,...  20 us
    unnamed x1, local copies, waits for them, and re-layouts  0.8 us

profile of v5, /device:TPU:1, one launch (start us, length us, event | category | flops | bytes accessed | tf_op | source)
XLA Modules:
  0.0 20.8 jit_solution(12091482939264696685)
XLA Ops:
  0.0 20.0 %mixer.1 = bf16[128,2048]{1,0:T(8,128)(2,1)S(1)} custom-call(bf16[256,512]{1,0:T(8,128)(2,1)} %refs_0_.1, f32[32,64]{1,0:T(8,128)} %refs_1_.1, f32[32,64]{1,0:T(8,128)} %refs_2_.1, f32[1,32]{1,0:T(1,128)} %bitcast.11, f32[32,16,64]{2,1,0:T(8,128)} %bitcast.6, f32[32,16,64]{2,1,0:T(8,128)} %bitcast.7, f32[32,16,64]{2,1,0:T(8,128)} %refs_6_.1, ...), custom_call_target="tpu_custom_call" | custom-call | tf_op jit(solution)/shard_map/mixer/pallas_call | solution.py:534
  20.0 0.8 %copy.15 = bf16[128,2048]{1,0:T(8,128)(2,1)} copy(bf16[128,2048]{1,0:T(8,128)(2,1)S(1)} %mixer.1) | data formatting | bytes 1048576

commit v6 on v5

--- a/solution.py
+++ b/solution.py
@@ -40,7 +40,7 @@
     (x_h, lr_h, li_h, ls_h, br_h, bi_h, cr_h, ci_h, sk_h, vw_h, gw_h, vb_h, gb_h, out_ref,
      x_v, ls_v, lam_v, b_v, c_v, sk_v, bias_v, w_v,
      xp_v, bmat_v, mats_v, keep_v, zr_v, zi_v, zcat_v, wcat_v, gain_v, resp_v, both_v, act_v,
-     par_v, fin_v, tab_x, tab_y, sum_v, end_v, row_v, plane_v, recv_x, recv_y, recv_z, h_v, pass_v,
+     par_v, fin_v, tab_x, tab_y, tab_z, sum_v, end_v, row_v, plane_v, recv_x, recv_y, recv_z, h_v, pass_v,
      sems, got_sems, ready) = refs
     me = lax.axis_index("sp")
     core = lax.axis_index("tp")
@@ -59,7 +59,7 @@
     per = 128 // state
 
     (s_step, s_lam, s_x, s_b, s_c, s_skip, s_bias, s_w, s_h) = (sems.at[i] for i in range(9))
-    (g_x, g_y, g_z, g_par, g_gain, g_resp, g_h, g_w0, g_w1) = (got_sems.at[i] for i in range(9))
+    (g_x, g_y, g_z, g_par, g_gain, g_resp, g_h, g_w) = (got_sems.at[i] for i in range(8))
 
     def settle(ref, sem):
         pltpu.make_async_copy(ref, ref, sem).wait()
@@ -67,8 +67,9 @@
     quarter = rows // 4
     moves = [(ls_h, ls_v, s_step), (lr_h, lam_v.at[0], s_lam), (li_h, lam_v.at[1], s_lam)]
     moves += [(x_h.at[pl.ds(i * quarter, quarter)], x_v.at[pl.ds(i * quarter, quarter)], s_x) for i in range(4)]
-    moves += [(br_h, b_v.at[0], s_b), (bi_h, b_v.at[1], s_b), (cr_h, c_v.at[0], s_c), (ci_h, c_v.at[1], s_c)]
-    moves += [(sk_h, sk_v, s_skip), (vb_h, bias_v.at[0], s_bias), (gb_h, bias_v.at[1], s_bias)]
+    moves += [(br_h, b_v.at[0], s_b), (bi_h, b_v.at[1], s_b)]
+    later = [(cr_h, c_v.at[0], s_c), (ci_h, c_v.at[1], s_c), (sk_h, sk_v, s_skip)]
+    later += [(vb_h, bias_v.at[0], s_bias), (gb_h, bias_v.at[1], s_bias)]
     for src, dst, sem in moves:
         pltpu.make_async_copy(src, dst, sem).start()
     depth = vw_h.shape[0]
@@ -86,9 +87,10 @@
             src_ref=src, dst_ref=dst, send_sem=sent, recv_sem=got,
             device_id=(me, other_core), device_id_type=MESH)
 
-    wcols = [pl.ds(i * (width // 2), width // 2) for i in range(2)]
-    out_w = [[across(s.at[:, cols], w_v.at[i, place_of(core), cols], s_c, got) for i, s in enumerate(weights)]
-             for cols, got in zip(wcols, (g_w0, g_w1))]
+    first = width // 4 * 3
+    wcols = [pl.ds(0, first), pl.ds(first, width - first)]
+    out_w = [[across(s.at[:, cols], w_v.at[i, place_of(core), cols], s_c, g_w) for i, s in enumerate(weights)]
+             for cols in wcols]
     out_par, got_par = (across(par_v.at[i], par_v.at[i], s_lam, g_par) for i in (core, other_core))
     out_gain, got_gain = (across(gain_v.at[i], gain_v.at[i], s_b, g_gain) for i in (core, other_core))
     out_resp = across(resp_v.at[rows_of(other_core)], both_v.at[core], s_bias, g_resp)
@@ -184,6 +186,8 @@
 
     settle(x_v, s_x)
     settle(b_v, s_b)
+    for src, dst, sem in later:
+        pltpu.make_async_copy(src, dst, sem).start()
     late = 1 + (half.bit_length() - 1)
     for g in range(groups):
         b, l = g // gpb, g % gpb
@@ -200,17 +204,22 @@
         cols = slice(b * 128, (b + 1) * 128)
         both = jnp.concatenate([x_v[:half, cols], x_v[half:, cols]], axis=1)
         out = jnp.dot(both, bmat_v[b], preferred_element_type=F32)
-        e_r, e_i = power(8, b)
-        z_r, z_i = out[:8, :lanes], out[:8, lanes:]
+        zr_v[b, :half] = out[:, :lanes]
+        zi_v[b, :half] = out[:, lanes:]
+    for which in [(b, b + 1) for b in range(0, blocks, 2)]:
+        each = [power(8, b) for b in which]
+        value = [(zr_v[b, :8], zi_v[b, :8]) for b in which]
         for k in range(1, half // 8):
-            p_r, p_i = cmul(e_r, e_i, z_r, z_i)
-            z_r, z_i = p_r + out[8 * k:8 * k + 8, :lanes], p_i + out[8 * k:8 * k + 8, lanes:]
-        v_r, v_i = cmul(*eight(b, True), z_r, z_i)
-        v_r, v_i = jnp.sum(v_r, axis=0, keepdims=True), jnp.sum(v_i, axis=0, keepdims=True)
-        for u in range(fold):
-            at, cols = b * fold + u, slice(u * wide, (u + 1) * wide)
-            fin_v[at:at + 1] = v_r[:, cols]
-            fin_v[tall + at:tall + at + 1] = v_i[:, cols]
+            here = pl.ds(8 * k, 8)
+            moved = [cmul(*e, *v) for e, v in zip(each, value)]
+            value = [(m_r + zr_v[b, here], m_i + zi_v[b, here]) for b, (m_r, m_i) in zip(which, moved)]
+        for b, v in zip(which, value):
+            v_r, v_i = cmul(*eight(b, True), *v)
+            v_r, v_i = jnp.sum(v_r, axis=0, keepdims=True), jnp.sum(v_i, axis=0, keepdims=True)
+            for u in range(fold):
+                at, cols = b * fold + u, slice(u * wide, (u + 1) * wide)
+                fin_v[at:at + 1] = v_r[:, cols]
+                fin_v[tall + at:tall + at + 1] = v_i[:, cols]
     end_v[...] = fin_v[...].astype(BF16)
 
     def to_row(k):
@@ -253,7 +262,7 @@
         @pl.loop(0, z)
         def _(d):
             pl.semaphore_signal(
-                ready.at[z], inc=1, device_id=(peer(*lines[2], d - z + nz)[1], lead), device_id_type=MESH)
+                ready, inc=1, device_id=(peer(*lines[2], d - z + nz)[1], lead), device_id_type=MESH)
 
     @pl.when(core != lead)
     def _():
@@ -386,54 +395,61 @@
     for b in range(0, blocks, 2):
         carry_powers(core, (b, b + 1))
 
-    @pl.when(core == lead)
-    def _():
-        settle(recv_y.at[pl.ds(0, ny - 1)], g_y)
-        t_r, t_i, y_r, y_i = collect(1, tab_y, sum_v[0], sum_v[1], functools.partial(from_line, 1))
-        plane_v[:span], plane_v[span:] = t_r.astype(BF16), t_i.astype(BF16)
-
-        @pl.loop(z + 1, nz)
-        def _(d):
-            pl.semaphore_wait(ready.at[d], 1)
-            along(2, d - z).start()
-
-        m_r, m_i = weight(tab_x, nx + x, y_r, y_i)
-        sum_v[2], sum_v[3] = sum_v[2] + m_r, sum_v[3] + m_i
-        sum_v[0], sum_v[1] = weight(tab_x, nx + x, tab_y[ny + y, :span], tab_y[ny + y, span:])
+    respond(blocks - 1)
+    out_resp.start()
+
+    @pl.when(core != lead)
+    def _():
+        for c in out_w[1]:
+            c.start()
+
+    both_v[core] = resp_v[rows_of(core), :]
+    for b in range(0, blocks, 2):
+        carry_powers(other_core, (b, b + 1))
 
     def hand_on(h_r, h_i):
         pass_v[:span], pass_v[span:] = h_r, h_i
         out_h.start()
         h_v[:span], h_v[span:] = cmul(*pair(late), h_r, h_i)
 
-    @pl.when((core == lead) & (z == 0))
-    def _():
-        hand_on(sum_v[2], sum_v[3])
-
-    respond(blocks - 1)
-    out_resp.start()
-
-    @pl.when(core != lead)
-    def _():
-        for c in out_w[1]:
-            c.start()
-
-    both_v[core] = resp_v[rows_of(core), :]
-    for b in range(0, blocks, 2):
-        carry_powers(other_core, (b, b + 1))
-
-    @pl.when((core == lead) & (z > 0))
-    def _():
-        settle_some(recv_z, g_z, z, nz)
-
-        def gather(k, carry):
-            h_r, h_i, p_r, p_i = carry
-            _, v_r, v_i = from_line(2, nz - 1 - k)
-            m_r, m_i = cmul(p_r, p_i, v_r, v_i)
-            return (h_r + m_r, h_i + m_i) + cmul(p_r, p_i, sum_v[4], sum_v[5])
-
-        h_r, h_i, _, _ = lax.fori_loop(0, z, gather, (sum_v[2], sum_v[3], sum_v[0], sum_v[1]))
-        hand_on(h_r, h_i)
+    @pl.when(core == lead)
+    def _():
+        s_r, s_i = weight(tab_x, nx + x, tab_y[ny + y, :span], tab_y[ny + y, span:])
+        for i in range(nz - 1):
+            tab_z[i, :span], tab_z[i, span:] = s_r, s_i
+            s_r, s_i = cmul(s_r, s_i, sum_v[4], sum_v[5])
+        settle(recv_y.at[pl.ds(0, ny - 1)], g_y)
+        t_r, t_i, y_r, y_i = collect(1, tab_y, sum_v[0], sum_v[1], functools.partial(from_line, 1))
+        plane_v[:span], plane_v[span:] = t_r.astype(BF16), t_i.astype(BF16)
+
+        @pl.when(z < nz - 1)
+        def _():
+            pl.semaphore_wait(ready, nz - 1 - z)
+
+        @pl.loop(0, nz - 1 - z)
+        def _(i):
+            d = jnp.where(z >= nz // 2, nz - 1 - i, z + 1 + i)
+            along(2, d - z).start()
+
+        m_r, m_i = weight(tab_x, nx + x, y_r, y_i)
+        h_r, h_i = sum_v[2] + m_r, sum_v[3] + m_i
+        sum_v[2], sum_v[3] = h_r, h_i
+
+        @pl.when(z == 0)
+        def _():
+            hand_on(h_r, h_i)
+
+        @pl.when(z > 0)
+        def _():
+            settle_some(recv_z, g_z, z, nz)
+
+            def gather(k, carry):
+                h_r, h_i = carry
+                _, v_r, v_i = from_line(2, nz - 1 - k)
+                m_r, m_i = weight(tab_z, k, v_r, v_i)
+                return h_r + m_r, h_i + m_i
+
+            hand_on(*lax.fori_loop(0, z, gather, (sum_v[2], sum_v[3])))
 
     @pl.when(core != lead)
     def _():
@@ -452,12 +468,10 @@
             total = nt_dot(wcat_v[i, b], keep_v[i, b]) + both_v[i, :, col]
             act_v[:, pl.ds(i * depth + b * 128, 128)] = jax.nn.gelu(total).astype(BF16)
     settle(w_v.at[:, place_of(core)], s_w)
-    settle(w_v.at[:, place_of(other_core), wcols[0]], g_w0)
+    settle(w_v.at[:, place_of(other_core)], g_w)
     piece = min(512, width)
     for j in range(width // piece):
         col = pl.ds(j * piece, piece)
-        if j * piece == width // 2:
-            settle(w_v.at[:, place_of(other_core), wcols[1]], g_w1)
         sums = [bias_v[i, :, col] + jnp.dot(act_v[...], w_v[i, :, col], preferred_element_type=F32) for i in range(2)]
         out_ref[:, col] = (sums[0] * jax.nn.sigmoid(sums[1])).astype(BF16)
     settle(w_v.at[:, place_of(core)], s_c)
@@ -518,6 +532,7 @@
         pltpu.VMEM(held, F32),
         pltpu.VMEM((2 * nx,) + pairs, F32),
         pltpu.VMEM((2 * ny,) + pairs, F32),
+        pltpu.VMEM((nz - 1,) + pairs, F32),
         pltpu.VMEM((6, pairs[0] // 2, pairs[1]), F32),
         pltpu.VMEM(held, BF16),
         pltpu.VMEM(pairs, BF16),
@@ -528,8 +543,8 @@
         pltpu.VMEM(pairs, F32),
         pltpu.VMEM(pairs, F32),
         pltpu.SemaphoreType.DMA((9,)),
-        pltpu.SemaphoreType.DMA((9,)),
-        pltpu.SemaphoreType.REGULAR((nz,)),
+        pltpu.SemaphoreType.DMA((8,)),
+        pltpu.SemaphoreType.REGULAR,
     ]
     return pl.pallas_call(
         functools.partial(kernel, ring, ntp, (rows, groups, state, size, width)),

time: 20.9 us -> 20.4 us (0.976); the launches traced: 20.8 us -> 20.1 us
  Pallas kernels: 20 us -> 19.3 us
    pallas_call x1, Pallas kernels: 20 us -> 19.3 us  [local(): pl.pallas_call(functools.partial(kernel, ring, ntp, (rows, groups, state,...]
where the time goes in v6:
time: 20.4 us; the launch traced here: 20.1 us
  Pallas kernels  19.3 us (95%)
  local copies, waits for them, and re-layouts  0.8 us (4%)
    pallas_call x1, Pallas kernels, local(): pl.pallas_call(functools.partial(kernel, ring, ntp, (rows, groups, state,...  19.3 us
    unnamed x1, local copies, waits for them, and re-layouts  0.8 us

profile of v6, /device:TPU:1, one launch (start us, length us, event | category | flops | bytes accessed | tf_op | source)
XLA Modules:
  0.0 20.1 jit_solution(9029281754892163760)
XLA Ops:
  0.0 19.3 %mixer.1 = bf16[128,2048]{1,0:T(8,128)(2,1)S(1)} custom-call(bf16[256,512]{1,0:T(8,128)(2,1)} %refs_0_.1, f32[32,64]{1,0:T(8,128)} %refs_1_.1, f32[32,64]{1,0:T(8,128)} %refs_2_.1, f32[1,32]{1,0:T(1,128)} %bitcast.11, f32[32,16,64]{2,1,0:T(8,128)} %bitcast.6, f32[32,16,64]{2,1,0:T(8,128)} %bitcast.7, f32[32,16,64]{2,1,0:T(8,128)} %refs_6_.1, ...), custom_call_target="tpu_custom_call" | custom-call | tf_op jit(solution)/shard_map/mixer/pallas_call | solution.py:549
  19.3 0.8 %copy.15 = bf16[128,2048]{1,0:T(8,128)(2,1)} copy(bf16[128,2048]{1,0:T(8,128)(2,1)S(1)} %mixer.1) | data formatting | bytes 1048576

commit v7 on v6

--- a/solution.py
+++ b/solution.py
@@ -200,26 +200,31 @@
             bmat_v[b, base + at:base + at + size, cols:cols + 128] = v_r.astype(BF16)
             bmat_v[b, base + at:base + at + size, lanes + cols:lanes + cols + 128] = v_i.astype(BF16)
 
-    for b in range(blocks):
+    def fold_halves(b):
         cols = slice(b * 128, (b + 1) * 128)
         both = jnp.concatenate([x_v[:half, cols], x_v[half:, cols]], axis=1)
         out = jnp.dot(both, bmat_v[b], preferred_element_type=F32)
         zr_v[b, :half] = out[:, :lanes]
         zi_v[b, :half] = out[:, lanes:]
-    for which in [(b, b + 1) for b in range(0, blocks, 2)]:
-        each = [power(8, b) for b in which]
-        value = [(zr_v[b, :8], zi_v[b, :8]) for b in which]
-        for k in range(1, half // 8):
-            here = pl.ds(8 * k, 8)
-            moved = [cmul(*e, *v) for e, v in zip(each, value)]
-            value = [(m_r + zr_v[b, here], m_i + zi_v[b, here]) for b, (m_r, m_i) in zip(which, moved)]
-        for b, v in zip(which, value):
-            v_r, v_i = cmul(*eight(b, True), *v)
-            v_r, v_i = jnp.sum(v_r, axis=0, keepdims=True), jnp.sum(v_i, axis=0, keepdims=True)
-            for u in range(fold):
-                at, cols = b * fold + u, slice(u * wide, (u + 1) * wide)
-                fin_v[at:at + 1] = v_r[:, cols]
-                fin_v[tall + at:tall + at + 1] = v_i[:, cols]
+
+    fold_halves(0)
+    for b in range(blocks):
+        if b + 1 < blocks:
+            fold_halves(b + 1)
+        e_r, e_i = power(8, b)
+        part = half // 2
+        value = [(zr_v[b, i * part:i * part + 8], zi_v[b, i * part:i * part + 8]) for i in range(2)]
+        for k in range(1, part // 8):
+            moved = [cmul(e_r, e_i, *v) for v in value]
+            value = [(m_r + zr_v[b, i * part + 8 * k:i * part + 8 * k + 8], m_i + zi_v[b, i * part + 8 * k:i * part + 8 * k + 8])
+                     for i, (m_r, m_i) in enumerate(moved)]
+        m_r, m_i = cmul(*power(part, b), *value[0])
+        v_r, v_i = cmul(*eight(b, True), m_r + value[1][0], m_i + value[1][1])
+        v_r, v_i = jnp.sum(v_r, axis=0, keepdims=True), jnp.sum(v_i, axis=0, keepdims=True)
+        for u in range(fold):
+            at, cols = b * fold + u, slice(u * wide, (u + 1) * wide)
+            fin_v[at:at + 1] = v_r[:, cols]
+            fin_v[tall + at:tall + at + 1] = v_i[:, cols]
     end_v[...] = fin_v[...].astype(BF16)
 
     def to_row(k):

time: 20.4 us -> 20.2 us (level); the launches traced: 20.1 us -> 20.1 us
  no operation moved by 1% of the time
where the time goes in v7:
time: 20.2 us; the launch traced here: 20.1 us
  Pallas kernels  19.3 us (96%)
  local copies, waits for them, and re-layouts  0.8 us (4%)
    pallas_call x1, Pallas kernels, local(): pl.pallas_call(functools.partial(kernel, ring, ntp, (rows, groups, state,...  19.3 us
    unnamed x1, local copies, waits for them, and re-layouts  0.8 us

profile of v7, /device:TPU:1, one launch (start us, length us, event | category | flops | bytes accessed | tf_op | source)
XLA Modules:
  0.0 20.1 jit_solution(7717739127510781692)
XLA Ops:
  0.0 19.3 %mixer.1 = bf16[128,2048]{1,0:T(8,128)(2,1)S(1)} custom-call(bf16[256,512]{1,0:T(8,128)(2,1)} %refs_0_.1, f32[32,64]{1,0:T(8,128)} %refs_1_.1, f32[32,64]{1,0:T(8,128)} %refs_2_.1, f32[1,32]{1,0:T(1,128)} %bitcast.11, f32[32,16,64]{2,1,0:T(8,128)} %bitcast.6, f32[32,16,64]{2,1,0:T(8,128)} %bitcast.7, f32[32,16,64]{2,1,0:T(8,128)} %refs_6_.1, ...), custom_call_target="tpu_custom_call" | custom-call | tf_op jit(solution)/shard_map/mixer/pallas_call | solution.py:554
  19.3 0.8 %copy.15 = bf16[128,2048]{1,0:T(8,128)(2,1)} copy(bf16[128,2048]{1,0:T(8,128)(2,1)S(1)} %mixer.1) | data formatting | bytes 1048576
